TPU v7x, 256 devices: a whole 4x4x8 slice. The times are simulated.
256 devices in a mesh: st: 16 (over y, x), tp: 16 (over z, core).
Axes of the slice: x: 4, y: 4, z: 8, core: 2. Of those that a mesh axis runs over, the one named last changes fastest.
Arguments:
- normed: bfloat16 [8192, 2048], P('st'), may hold values from -128 to 128
- store: bfloat16 [32768, 2048], P('st'), may hold values from -5 to 5
- passage_ids: int32 [64, 2], P('st'), may hold values from 0 to 511, as said below
- w_query: bfloat16 [2048, 2048], P(None, 'tp'), as said below
- w_gate: bfloat16 [2048, 2048], P(None, 'tp'), may hold values from -0.125 to 0.125
- w_key: bfloat16 [2048, 2048], P(None, 'tp'), as said below
- w_value: bfloat16 [2048, 2048], P(None, 'tp'), may hold values from -0.125 to 0.125
- cotangent: bfloat16 [8192, 2048], P('st', 'tp'), may hold values from -6 to 6
Outputs:
- grad_rows: float32 [8192, 2048], P('st', 'tp')
- grad_store: float32 [32768, 2048], P('st', 'tp')
- grad_query_weight: float32 [2048, 2048], P('st', 'tp')
Inputs may be any that keep to these rules, and one draw needn't show every extreme that they name: `passage_ids`: each row names 2 passages. The passages read by the blocks of one index of st are all different, and at most 1 of them belong to any one owner (the owner of passage p is the index p // 32 of st). In every draw some owner has one of its passages read by every index of st. `w_query`: entries lie within 6 * 2048 ** -0.5 in magnitude. `w_key`: entries lie within 8 * 2048 ** -0.5 in magnitude.
All inputs are finite; a program needn't handle non-finite values.
Results may differ from a plain program's by a relative error of at most 0.019.
Values may be sent and summed in bfloat16 or wider, within the bound.
No kernel may reach another device: no remote copies, remote signals or barrier semaphores. Data moves between devices by JAX's collectives and lax.ppermute only.
A program may use at most 128 MiB of HBM per device.

v0:
```python
import jax
import jax.numpy as jnp
from jax import lax
from jax.sharding import PartitionSpec as P

DH = 128
BLK = 128
PLEN = 64


def in_blocks(array, dim, length):
    before, after = (array.shape[:dim], array.shape[dim + 1 :])
    return jnp.moveaxis(array.reshape(*before, length, -1, *after), dim, 0)


def summed_on_arrival(array, axis, dim):
    length = lax.axis_size(axis)
    blocks = lax.all_to_all(in_blocks(array, dim, length), axis, 0, 0, tiled=True)
    return jnp.sum(blocks.astype(jnp.float32), axis=0)


def side_by_side(arrays, axis, dim, along):
    ends, at = ([], 0)
    for a in arrays[:-1]:
        at += a.shape[along]
        ends.append(at)
    both = jnp.concatenate(arrays, axis=along)
    return tuple(
        jnp.split(lax.psum_scatter(both, axis, scatter_dimension=dim, tiled=True), ends, axis=along)
    )


def shards(normed, store, passage_ids, w_query, w_gate, w_key, w_value, cotangent):
    peer_count = lax.axis_size("st")
    blocks = passage_ids.shape[0]
    read_count = passage_ids.shape[1]
    requests = blocks * read_count
    slot_most = max(1, 2 * requests // peer_count)
    slot_count = peer_count * slot_most
    tok_rows = normed.shape[0]
    head_width = w_query.shape[1]
    heads_dev = head_width // DH
    pass_dev = store.shape[0] // PLEN
    key_span = read_count * PLEN
    score_scale = DH ** (-0.5)
    flat_ids = passage_ids.reshape(requests)
    owners = flat_ids // pass_dev
    local_ids = flat_ids % pass_dev
    positions = jnp.arange(requests, dtype=jnp.int32)
    before = (owners[:, None] == owners[None, :]) & (positions[None, :] < positions[:, None])
    rank_among = jnp.sum(before.astype(jnp.int32), axis=1)
    slot_of = owners * slot_most + rank_among
    slot_hit = slot_of[:, None] == jnp.arange(slot_count, dtype=jnp.int32)[None, :]
    slot_table = jnp.max(jnp.where(slot_hit, local_ids[:, None], -1), axis=0)
    wanted = lax.all_to_all(
        slot_table.reshape(peer_count, slot_most), "st", split_axis=0, concat_axis=0, tiled=True
    )
    w_pair = jnp.concatenate([w_key, w_value], axis=1)
    projected = jnp.dot(store, w_pair, preferred_element_type=jnp.float32).astype(jnp.bfloat16)
    projected = projected.reshape(pass_dev, PLEN, 2 * head_width)
    served_ids = wanted.reshape(slot_count)
    served = jnp.take(projected, jnp.maximum(served_ids, 0), axis=0)
    served = jnp.where((served_ids >= 0)[:, None, None], served, jnp.zeros_like(served))
    arrived = lax.all_to_all(
        served.reshape(peer_count, slot_most, PLEN, 2 * head_width),
        "st",
        split_axis=0,
        concat_axis=0,
        tiled=True,
    )
    queries = jnp.dot(normed, w_query, preferred_element_type=jnp.float32).astype(jnp.bfloat16)
    gate_open = jax.nn.sigmoid(jnp.dot(normed, w_gate, preferred_element_type=jnp.float32))
    picked = jnp.take(arrived.reshape(slot_count, PLEN, 2 * head_width), slot_of, axis=0)
    picked = picked.reshape(blocks, key_span, 2, heads_dev, DH)
    key_rows = picked[:, :, 0]
    value_rows = picked[:, :, 1]
    q_blocks = queries.reshape(blocks, BLK, heads_dev, DH)
    scores = (
        jnp.einsum("bthd,bshd->bhts", q_blocks, key_rows, preferred_element_type=jnp.float32)
        * score_scale
    )
    attn_probs = jax.nn.softmax(scores, axis=-1)
    probs_low = attn_probs.astype(jnp.bfloat16)
    attended = jnp.einsum(
        "bhts,bshd->bthd", probs_low, value_rows, preferred_element_type=jnp.float32
    )
    gate_blocks = gate_open.reshape(blocks, BLK, heads_dev, DH)
    upstream = cotangent.astype(jnp.float32).reshape(blocks, BLK, heads_dev, DH)
    d_attended = (upstream * gate_blocks).astype(jnp.bfloat16)
    d_gate = (upstream * attended * gate_blocks * (1.0 - gate_blocks)).astype(jnp.bfloat16)
    d_gate = d_gate.reshape(tok_rows, head_width)
    d_values = jnp.einsum(
        "bhts,bthd->bshd", probs_low, d_attended, preferred_element_type=jnp.float32
    ).astype(jnp.bfloat16)
    d_probs = jnp.einsum(
        "bthd,bshd->bhts", d_attended, value_rows, preferred_element_type=jnp.float32
    )
    row_delta = jnp.sum(d_probs * attn_probs, axis=-1, keepdims=True)
    d_scores = (attn_probs * (d_probs - row_delta) * score_scale).astype(jnp.bfloat16)
    d_query = (
        jnp.einsum("bhts,bshd->bthd", d_scores, key_rows, preferred_element_type=jnp.float32)
        .astype(jnp.bfloat16)
        .reshape(tok_rows, head_width)
    )
    d_keys = jnp.einsum(
        "bhts,bthd->bshd", d_scores, q_blocks, preferred_element_type=jnp.float32
    ).astype(jnp.bfloat16)
    d_pair = jnp.stack([d_keys, d_values], axis=2).reshape(requests, PLEN, 2 * head_width)
    row_part = jnp.dot(d_query, w_query.T, preferred_element_type=jnp.float32)
    row_part = row_part + jnp.dot(d_gate, w_gate.T, preferred_element_type=jnp.float32)
    grad_query_weight = summed_on_arrival(
        lax.dot_general(
            normed, d_query, (((0,), (0,)), ((), ())), preferred_element_type=jnp.float32
        ).astype(jnp.bfloat16),
        "st",
        0,
    )
    owned = (jnp.arange(pass_dev, dtype=jnp.int32)[:, None] == served_ids[None, :]).astype(
        jnp.float32
    )
    per_request = jnp.dot(
        d_pair.reshape(requests * PLEN, 2 * head_width),
        w_pair.T,
        preferred_element_type=jnp.float32,
    )
    grad_rows, slice_part = tuple(
        (
            part.astype(jnp.float32)
            for part in side_by_side(
                (row_part.astype(jnp.bfloat16), per_request.astype(jnp.bfloat16)), "tp", 1, 0
            )
        )
    )
    slice_cols = slice_part.shape[1]
    outgoing = lax.dot_general(
        slot_hit.astype(jnp.float32),
        slice_part.reshape(requests, PLEN * slice_cols),
        (((0,), (0,)), ((), ())),
        precision=lax.Precision.HIGHEST,
    )
    returned = lax.all_to_all(
        outgoing.reshape(peer_count, slot_most, PLEN, slice_cols).astype(jnp.bfloat16),
        "st",
        split_axis=0,
        concat_axis=0,
        tiled=True,
    ).astype(jnp.float32)
    grad_store = jnp.dot(
        owned, returned.reshape(slot_count, PLEN * slice_cols), precision=lax.Precision.HIGHEST
    ).reshape(pass_dev * PLEN, slice_cols)
    return (grad_rows, grad_store, grad_query_weight)


def solution(mesh):
    placed = (
        P("st", None),
        P("st", None),
        P("st", None),
        P(None, "tp"),
        P(None, "tp"),
        P(None, "tp"),
        P(None, "tp"),
        P("st", "tp"),
    )
    return jax.shard_map(
        shards,
        mesh=mesh,
        in_specs=placed,
        out_specs=(P("st", "tp"), P("st", "tp"), P("st", "tp")),
        check_vma=False,
    )
```

profile of v0, /device:TPU:2, one launch (start us, length us, event | category | flops | bytes accessed | tf_op | source)
XLA Modules:
  0.0 169.7 jit_solution(13554265546349603873)
XLA Ops:
  9.2 7.5 %all-to-all-start = ((s32[16,1,1]{2,1,0:T(1,128)}), s32[16,1,1]{2,1,0:T(1,128)S(1)}, u32[]{:S(2)}, u32[]{:S(2)}) async-start(s32[16,1,1]{2,1,0:T(1,128)} %copy.86), calls=%async_computation | async-start | bytes 16384 | tf_op jit(solution)/shard_map/all_to_all | solution.py:55
  18.0 1.2 constant_dynamic-update-slice_fusion
  19.1 6.8 %fusion.2 = bf16[2048,256]{0,1:T(8,128)(2,1)} fusion(bf16[2048,256]{1,0:T(8,128)(2,1)S(1)} %constant_dynamic-update-slice_fusion, bf16[2048,2048]{1,0:T(8,128)(2,1)} %param.9), kind=kOutput, calls=%fused_computation.8 | convolution fusion | flops 2148007936 | bytes 10485760 | tf_op jit(solution)/shard_map/dot_general | solution.py:59
  26.0 1.4 convolution_convert_fusion.4
  27.3 2.3 %copy.87 = bf16[2048,256]{1,0:T(8,128)(2,1)} copy(bf16[2048,256]{0,1:T(8,128)(2,1)} %fusion.2) | data formatting | bytes 2097152 | tf_op jit(solution)/shard_map/convert_element_type | solution.py:59
  30.3 2.6 %gather_fusion = bf16[16,64,256]{2,1,0:T(8,128)(2,1)} fusion(bf16[32,64,256]{2,1,0:T(8,128)(2,1)} %bitcast.115, s32[1024]{0:T(1024)S(1)} %pad_clamp_fusion.1), kind=kCustom, calls=%fused_computation | custom fusion | bytes 1048640 | tf_op jit(solution)/shard_map/jit(_take)/gather | solution.py:62
  33.3 2.0 %fusion.21 = bf16[16,1,64,256]{3,2,1,0:T(8,128)(2,1)} fusion(bf16[16,64,256]{2,1,0:T(8,128)(2,1)} %gather_fusion, pred[16]{0:T(512)(128)(4,1)S(1)} %maximum_compare_fusion, pred[16]{0:T(512)(128)(4,1)S(1)} %compare_reduce_fusion), kind=kLoop, calls=%fused_computation.39 | loop fusion | flops 524288 | bytes 1048608 | tf_op jit(solution)/shard_map/jit(_where)/select_n | solution.py:63
  35.2 7.2 %all-to-all-start.1 = ((bf16[16,1,64,256]{3,2,1,0:T(8,128)(2,1)}), bf16[16,1,64,256]{3,2,1,0:T(8,128)(2,1)}, u32[]{:S(2)}, u32[]{:S(2)}) async-start(bf16[16,1,64,256]{3,2,1,0:T(8,128)(2,1)} %fusion.21), calls=%async_computation.1 | async-start | bytes 1048576 | tf_op jit(solution)/shard_map/all_to_all | solution.py:64
  42.7 2.5 %multiply_convert_fusion = (bf16[512,128]{1,0:T(8,128)(2,1)S(1)}, f32[512,128]{1,0:T(8,128)}) fusion(bf16[512,128]{1,0:T(8,128)(2,1)S(1)} %copy-done.7, bf16[512,2048]{1,0:T(8,128)(2,1)S(1)} %copy-done, bf16[2048,128]{1,0:T(8,128)(2,1)} %param.12), kind=kOutput, calls=%fused_computation.50 | convolution fusion | flops 268828672 | bytes 3145728 | tf_op jit(solution)/shard_map/dot_general | solution.py:72
  45.2 7.0 %all-to-all-done.1 = bf16[16,1,64,256]{3,2,1,0:T(8,128)(2,1)} async-done(((bf16[16,1,64,256]{3,2,1,0:T(8,128)(2,1)}), bf16[16,1,64,256]{3,2,1,0:T(8,128)(2,1)}, u32[]{:S(2)}, u32[]{:S(2)}) %all-to-all-start.1) | async-done | bytes 524320 | tf_op jit(solution)/shard_map/all_to_all | solution.py:64
  52.2 1.6 gather_fusion.1
  55.7 2.0 %fusion.54 = (f32[4,128]{1,0:T(4,128)S(1)}, f32[4,128,128]{1,2,0:T(8,128)}) fusion(bf16[4,128,128]{2,1,0:T(8,128)(2,1)} %bitcast.124, bf16[4,128,2,1,128]{4,1,0,3,2:T(8,128)(2,1)S(1)} %copy_select_fusion), kind=kOutput, calls=%fused_computation.106 | convolution fusion | flops 16973952 | bytes 526336 | tf_op jit(solution)/shard_map/sub | solution.py:82
  58.5 1.5 convolution_convert_fusion.7
  60.0 2.1 %fusion.18 = bf16[4,128,1,1,128]{1,4,0,3,2:T(8,128)(2,1)} fusion(bf16[4,128,128]{2,1,0:T(8,128)(2,1)} %bitcast.125, f32[4,128,128]{1,2,0:T(8,128)} %fusion.34, f32[4,128,128]{1,2,0:T(8,128)} %get-tuple-element.21, f32[4,128]{1,0:T(4,128)S(1)} %get-tuple-element.20), kind=kOutput, calls=%fused_computation.33 | convolution fusion | flops 17302144 | bytes 788480 | tf_op jit(solution)/shard_map/bhts,bthd->bshd/dot_general | solution.py:105
  62.1 1.3 fusion.19
  63.4 3.7 %fusion.55 = f32[512,2048]{1,0:T(8,128)} fusion(bf16[512,128]{1,0:T(8,128)(2,1)S(1)} %bitcast.118, bf16[2048,128]{1,0:T(8,128)(2,1)} %param.11), kind=kOutput, calls=%fused_computation.107 | convolution fusion | flops 268435456 | bytes 4849664 | tf_op jit(solution)/shard_map/dot_general | solution.py:109
  68.0 1.8 %convolution_convert_fusion = bf16[512,2048]{1,0:T(8,128)(2,1)S(1)} fusion(bf16[2048,256]{1,0:T(8,128)(2,1)S(1)} %constant_dynamic-update-slice_fusion, bf16[64,8,2,128]{3,2,1,0:T(2,128)(2,1)} %bitcast.117), kind=kOutput, calls=%fused_computation.6 | convolution fusion | flops 537919488 | bytes 3407872 | tf_op jit(solution)/shard_map/dot_general | solution.py:121
  69.9 1.4 fusion.16
  72.0 2.6 %pad_maximum_fusion = bf16[1024,2048]{1,0:T(8,128)(2,1)} fusion(bf16[512,2048]{1,0:T(8,128)(2,1)S(1)} %convolution_convert_fusion, bf16[512,2048]{1,0:T(8,128)(2,1)S(1)} %add_convert_fusion), kind=kLoop, calls=%fused_computation.4 | loop fusion | flops 8388608 | bytes 8388608 | tf_op jit(solution)/shard_map/concatenate | solution.py:27
  74.6 6.4 %copy.108 = bf16[1024,2048]{0,1:T(8,128)(2,1)} copy(bf16[1024,2048]{1,0:T(8,128)(2,1)} %pad_maximum_fusion) | data formatting | bytes 8388608
  82.4 4.8 %all-to-all-start.3 = ((bf16[16,128,128]{1,2,0:T(8,128)(2,1)}), bf16[16,128,128]{1,2,0:T(8,128)(2,1)S(1)}, u32[]{:S(2)}, u32[]{:S(2)}) async-start(bf16[16,128,128]{1,2,0:T(8,128)(2,1)} %bitcast.113), calls=%async_computation.3 | async-start | bytes 1048576 | tf_op jit(solution)/shard_map/all_to_all | solution.py:18
  87.2 57.3 %reduce-scatter.4.cloned.1.call-done = bf16[128,1024]{1,0:T(8,128)(2,1)} async-done(((bf16[2048,1024]{1,0:T(8,128)(2,1)}), bf16[128,1024]{1,0:T(8,128)(2,1)}) %reduce-scatter.4.cloned.1.call-update) | async-done | bytes 262160
  146.9 7.3 %all-to-all-start.2 = ((bf16[16,1,64,128]{3,2,1,0:T(8,128)(2,1)}), bf16[16,1,64,128]{3,2,1,0:T(8,128)(2,1)S(1)}, u32[]{:S(2)}, u32[]{:S(2)}) async-start(bf16[16,1,64,128]{3,2,1,0:T(8,128)(2,1)} %copy.98), calls=%async_computation.2 | async-start | bytes 524288 | tf_op jit(solution)/shard_map/all_to_all | solution.py:141
  155.8 5.7 %all-to-all-done.2 = bf16[16,1,64,128]{3,2,1,0:T(8,128)(2,1)S(1)} async-done(((bf16[16,1,64,128]{3,2,1,0:T(8,128)(2,1)}), bf16[16,1,64,128]{3,2,1,0:T(8,128)(2,1)S(1)}, u32[]{:S(2)}, u32[]{:S(2)}) %all-to-all-start.2) | async-done | bytes 262176 | tf_op jit(solution)/shard_map/all_to_all | solution.py:141
  (58 shorter events, 15.7 us)
Async XLA Ops:
  7.2 18.8 %copy-start = (bf16[512,2048]{1,0:T(8,128)(2,1)S(1)}, bf16[512,2048]{1,0:T(8,128)(2,1)}, u32[]{:S(2)}) copy-start(bf16[512,2048]{1,0:T(8,128)(2,1)} %param.8) | copy-start | bytes 6291460
  9.2 20.4 %all-to-all-start = ((s32[16,1,1]{2,1,0:T(1,128)}), s32[16,1,1]{2,1,0:T(1,128)S(1)}, u32[]{:S(2)}, u32[]{:S(2)}) async-start(s32[16,1,1]{2,1,0:T(1,128)} %copy.86), calls=%async_computation | async-start | bytes 16384 | tf_op jit(solution)/shard_map/all_to_all | solution.py:55
  19.1 6.8 %copy-start.2 = (bf16[2048,128]{1,0:T(8,128)(2,1)S(1)}, bf16[2048,128]{1,0:T(8,128)(2,1)}, u32[]{:S(2)}) copy-start(bf16[2048,128]{1,0:T(8,128)(2,1)} %param.11) | copy-start | bytes 1572868
  26.0 16.8 %copy-start.7 = (bf16[512,128]{1,0:T(8,128)(2,1)S(1)}, bf16[512,128]{1,0:T(8,128)(2,1)}, u32[]{:S(2)}) copy-start(bf16[512,128]{1,0:T(8,128)(2,1)} %param.15) | copy-start | bytes 393220
  35.2 16.9 %all-to-all-start.1 = ((bf16[16,1,64,256]{3,2,1,0:T(8,128)(2,1)}), bf16[16,1,64,256]{3,2,1,0:T(8,128)(2,1)}, u32[]{:S(2)}, u32[]{:S(2)}) async-start(bf16[16,1,64,256]{3,2,1,0:T(8,128)(2,1)} %fusion.21), calls=%async_computation.1 | async-start | bytes 1048576 | tf_op jit(solution)/shard_map/all_to_all | solution.py:64
  42.5 102.1 %reduce-scatter.4.cloned.1.call-start = ((), (), s32[]{:S(2)}) async-start(), calls=%async_computation.5 | async-start | bytes 4456448
  45.2 13.3 %copy-start.5 = (bf16[512,128]{1,0:T(8,128)(2,1)}, bf16[512,128]{1,0:T(8,128)(2,1)S(1)}, u32[]{:S(2)}) copy-start(bf16[512,128]{1,0:T(8,128)(2,1)S(1)} %get-tuple-element.18) | copy-start | bytes 393220
  55.7 7.8 %copy-start.3 = (bf16[4,128,2,1,128]{4,1,0,3,2:T(8,128)(2,1)}, bf16[4,128,2,1,128]{4,1,0,3,2:T(8,128)(2,1)S(1)}, u32[]{:S(2)}) copy-start(bf16[4,128,2,1,128]{4,1,0,3,2:T(8,128)(2,1)S(1)} %copy_select_fusion) | copy-start | bytes 786436
  62.1 5.0 %copy-start.6 = (bf16[4,128,1,1,128]{1,4,0,3,2:T(8,128)(2,1)S(1)}, bf16[4,128,1,1,128]{1,4,0,3,2:T(8,128)(2,1)}, u32[]{:S(2)}) copy-start(bf16[4,128,1,1,128]{1,4,0,3,2:T(8,128)(2,1)} %fusion.18) | copy-start | bytes 393220
  68.0 3.2 %copy-start.1 = (f32[512,2048]{1,0:T(8,128)S(1)}, f32[512,2048]{1,0:T(8,128)}, u32[]{:S(2)}) copy-start(f32[512,2048]{1,0:T(8,128)} %fusion.55) | copy-start | bytes 12582916
  68.0 3.3 %copy-start.4 = (bf16[2048,128]{1,0:T(8,128)(2,1)S(1)}, bf16[2048,128]{1,0:T(8,128)(2,1)}, u32[]{:S(2)}) copy-start(bf16[2048,128]{1,0:T(8,128)(2,1)} %param.12) | copy-start | bytes 1572868
  82.4 64.5 %all-to-all-start.3 = ((bf16[16,128,128]{1,2,0:T(8,128)(2,1)}), bf16[16,128,128]{1,2,0:T(8,128)(2,1)S(1)}, u32[]{:S(2)}, u32[]{:S(2)}) async-start(bf16[16,128,128]{1,2,0:T(8,128)(2,1)} %bitcast.113), calls=%async_computation.3 | async-start | bytes 1048576 | tf_op jit(solution)/shard_map/all_to_all | solution.py:18
  146.9 14.6 %all-to-all-start.2 = ((bf16[16,1,64,128]{3,2,1,0:T(8,128)(2,1)}), bf16[16,1,64,128]{3,2,1,0:T(8,128)(2,1)S(1)}, u32[]{:S(2)}, u32[]{:S(2)}) async-start(bf16[16,1,64,128]{3,2,1,0:T(8,128)(2,1)} %copy.98), calls=%async_computation.2 | async-start | bytes 524288 | tf_op jit(solution)/shard_map/all_to_all | solution.py:141
Sparse Core Ops, SparseCore 0:
  81.1 63.4 reduce-scatter.3
where the time goes:
time: 171 us; the launch traced here: 170 us
  waiting for transfers between devices  70.1 us (41%)
  matrix products  27.1 us (16%)
  starting transfers between devices  26.8 us (16%)
  local copies, waits for them, and re-layouts  23.7 us (14%)
  between operations  14.2 us (8%)
  other arithmetic  7.85 us (5%)
    unnamed x2, waiting for transfers between devices  57.4 us
    unnamed x22, local copies, waits for them, and re-layouts  9.45 us
    all_to_all x1, starting transfers between devices, shards(): lax.all_to_all(slot_table.reshape(peer_count, slot_most), 'st', split_axi...  7.48 us
    all_to_all x1, starting transfers between devices, shards(): lax.all_to_all(outgoing.reshape(peer_count, slot_most, PLEN, slice_cols)....  7.29 us
    all_to_all x1, starting transfers between devices, shards(): lax.all_to_all(served.reshape(peer_count, slot_most, PLEN, 2 * head_width...  7.22 us
    all_to_all x1, waiting for transfers between devices, shards(): lax.all_to_all(served.reshape(peer_count, slot_most, PLEN, 2 * head_width...  7.01 us
    dot_general x1, matrix products, shards(): jnp.dot(store, w_pair, preferred_element_type=jnp.float32)  6.8 us
    all_to_all x1, waiting for transfers between devices, shards(): lax.all_to_all(outgoing.reshape(peer_count, slot_most, PLEN, slice_cols)....  5.67 us
  transfers between devices with their start and end apart: 5, of which 3 were waited for; matrix products, arithmetic and copies ran while one was open for 12% of the time, Pallas kernels for 0%

commit v1 on v0

v1 whole, which is shorter than its diff:
```python
import functools

import jax
import jax.numpy as jnp
from jax import lax
from jax.experimental import pallas as pl
from jax.experimental.pallas import tpu as pltpu
from jax.sharding import PartitionSpec as P

DH = 128
BLK = 128
PLEN = 64
BF16 = jnp.bfloat16
F32 = jnp.float32

VMEM = pl.BlockSpec(memory_space=pltpu.VMEM)
SMEM = pl.BlockSpec(memory_space=pltpu.SMEM)


def nt(a, b):
    return lax.dot_general(a, b, (((1,), (1,)), ((), ())), preferred_element_type=F32)


def tn(a, b):
    return lax.dot_general(a, b, (((0,), (0,)), ((), ())), preferred_element_type=F32)


def nn(a, b):
    return lax.dot_general(a, b, (((1,), (0,)), ((), ())), preferred_element_type=F32)


def cost(flops, nbytes):
    return pl.CostEstimate(flops=flops, bytes_accessed=nbytes, transcendentals=0)


def project_body(x_ref, wa_ref, wb_ref, out_ref):
    pair = jnp.concatenate([wa_ref[...], wb_ref[...]], axis=1)
    out_ref[...] = nn(x_ref[...], pair).astype(BF16)


def project_rows(store, w_key, w_value, tile):
    rows, width = store.shape
    cols = w_key.shape[1]
    return pl.pallas_call(
        project_body,
        grid=(rows // tile,),
        in_specs=[
            pl.BlockSpec((tile, width), lambda i: (i, 0)),
            pl.BlockSpec((width, cols), lambda i: (0, 0)),
            pl.BlockSpec((width, cols), lambda i: (0, 0)),
        ],
        out_specs=pl.BlockSpec((tile, 2 * cols), lambda i: (i, 0)),
        out_shape=jax.ShapeDtypeStruct((rows, 2 * cols), BF16),
        cost_estimate=cost(4 * rows * width * cols, 2 * rows * width),
        name="project_store",
    )(store, w_key, w_value)


def query_body(x_ref, wa_ref, wb_ref, q_ref, g_ref):
    cols = wa_ref.shape[1]
    pair = jnp.concatenate([wa_ref[...], wb_ref[...]], axis=1)
    both = nn(x_ref[...], pair)
    q_ref[...] = both[:, :cols].astype(BF16)
    g_ref[...] = jax.nn.sigmoid(both[:, cols:])


def project_tokens(normed, w_query, w_gate, tile):
    rows, width = normed.shape
    cols = w_query.shape[1]
    return pl.pallas_call(
        query_body,
        grid=(rows // tile,),
        in_specs=[
            pl.BlockSpec((tile, width), lambda i: (i, 0)),
            pl.BlockSpec((width, cols), lambda i: (0, 0)),
            pl.BlockSpec((width, cols), lambda i: (0, 0)),
        ],
        out_specs=[pl.BlockSpec((tile, cols), lambda i: (i, 0))] * 2,
        out_shape=[
            jax.ShapeDtypeStruct((rows, cols), BF16),
            jax.ShapeDtypeStruct((rows, cols), F32),
        ],
        cost_estimate=cost(4 * rows * width * cols, 2 * rows * width),
        name="project_tokens",
    )(normed, w_query, w_gate)


def serve_body(wanted_ref, rows_ref, out_ref):
    for s in range(out_ref.shape[0]):
        out_ref[s] = rows_ref[jnp.maximum(wanted_ref[s], 0)]


def serve(wanted, projected):
    peers = wanted.shape[0]
    return pl.pallas_call(
        serve_body,
        in_specs=[SMEM, VMEM],
        out_specs=VMEM,
        out_shape=jax.ShapeDtypeStruct((peers,) + projected.shape[1:], BF16),
        cost_estimate=cost(1 << 20, 1 << 20),
        name="serve",
    )(wanted, projected)


def attend_body(owner_ref, q_ref, gate_ref, cot_ref, kv_ref, out_ref):
    scale = DH ** (-0.5)
    tokens = q_ref.shape[0]
    reads = BLK // PLEN
    for b in range(tokens // BLK):
        rows = slice(b * BLK, (b + 1) * BLK)
        kv = jnp.concatenate([kv_ref[owner_ref[reads * b + r]] for r in range(reads)], axis=0)
        keys, values = kv[:, :DH], kv[:, DH:]
        q = q_ref[rows, :]
        gate = gate_ref[rows, :]
        cot = cot_ref[rows, :].astype(F32)
        scores = nt(q, keys) * scale
        top = jnp.max(scores, axis=1, keepdims=True)
        grown = jnp.exp(scores - top)
        probs = grown / jnp.sum(grown, axis=1, keepdims=True)
        low = probs.astype(BF16)
        attended = nn(low, values)
        d_att = (cot * gate).astype(BF16)
        d_gate = (cot * attended * gate * (1.0 - gate)).astype(BF16)
        d_probs = nt(d_att, values)
        delta = jnp.sum(d_probs * probs, axis=1, keepdims=True)
        d_scores = (probs * (d_probs - delta) * scale).astype(BF16)
        out_ref[rows, :DH] = nn(d_scores, keys).astype(BF16)
        out_ref[rows, DH:] = d_gate
        reads_at = slice(tokens + b * BLK, tokens + (b + 1) * BLK)
        out_ref[reads_at, :DH] = tn(d_scores, q).astype(BF16)
        out_ref[reads_at, DH:] = tn(low, d_att).astype(BF16)


def attend(owners, queries, gate_open, cotangent, arrived):
    tokens = queries.shape[0]
    return pl.pallas_call(
        attend_body,
        in_specs=[SMEM, VMEM, VMEM, VMEM, VMEM],
        out_specs=VMEM,
        out_shape=jax.ShapeDtypeStruct((2 * tokens, 2 * DH), BF16),
        cost_estimate=cost(14 * tokens * DH * DH, 1 << 20),
        name="attend",
    )(owners, queries, gate_open, cotangent, arrived)


def weight_grad_body(d_ref, x_ref, out_ref):
    d_query = d_ref[: x_ref.shape[0], :DH]
    flipped = d_query.astype(F32).T.astype(BF16)
    for j in range(out_ref.shape[0] // 2):
        both = nn(flipped, x_ref[:, 2 * j * DH : 2 * (j + 1) * DH]).astype(BF16)
        out_ref[2 * j] = both[:, :DH]
        out_ref[2 * j + 1] = both[:, DH:]


def weight_grad(grads, normed):
    tokens, width = normed.shape
    return pl.pallas_call(
        weight_grad_body,
        in_specs=[VMEM, VMEM],
        out_specs=VMEM,
        out_shape=jax.ShapeDtypeStruct((width // DH, DH, DH), BF16),
        cost_estimate=cost(2 * tokens * width * DH, 2 * tokens * width),
        name="weight_grad",
    )(grads, normed)


def spread_body(steps, chips, mine_ref, other_ref, *refs):
    weights, outs = refs[:8], refs[8:]
    at = lax.axis_index("tp")
    core = lax.rem(at, 2)
    chip = lax.div(at, 2)
    tokens = mine_ref.shape[0] // 2
    for out_ref, step in zip(outs, steps):
        to = lax.rem(chip + step, chips) * 2 + core
        rows = pl.ds(pl.multiple_of(to * DH, DH), DH)
        part = [w[rows, :] for w in weights]
        for half in range(2):
            side = slice(half * tokens, (half + 1) * tokens)
            left = jnp.concatenate([mine_ref[side, :], other_ref[side, :]], axis=1)
            right = jnp.concatenate(
                [part[2 * half], part[2 * half + 1], part[4 + 2 * half], part[5 + 2 * half]], axis=1
            )
            out_ref[side, :] = nt(left, right).astype(BF16)


def spread(steps, chips, mine, other, weights):
    rows = mine.shape[0]
    return pl.pallas_call(
        functools.partial(spread_body, steps, chips),
        in_specs=[VMEM] * 10,
        out_specs=[VMEM] * len(steps),
        out_shape=[jax.ShapeDtypeStruct((rows, DH), BF16)] * len(steps),
        cost_estimate=cost(len(steps) * 8 * rows * DH * DH, 4 << 20),
        name="spread_" + "_".join(str(s) for s in steps),
    )(mine, other, *weights)


def finish_body(owner_ref, own_ref, left_ref, right_ref, rows_ref, slots_ref):
    tokens = rows_ref.shape[0]

    def total(at):
        return (
            own_ref[at, :].astype(F32) + left_ref[at, :].astype(F32) + right_ref[at, :].astype(F32)
        )

    rows_ref[...] = total(slice(0, tokens))
    slots_ref[...] = jnp.zeros_like(slots_ref)
    for i in range(tokens // PLEN):
        at = slice(tokens + i * PLEN, tokens + (i + 1) * PLEN)
        slots_ref[owner_ref[i]] = total(at).astype(BF16)


def finish(owners, own, left, right, peers):
    rows = own.shape[0]
    return pl.pallas_call(
        finish_body,
        in_specs=[SMEM, VMEM, VMEM, VMEM],
        out_specs=[VMEM, VMEM],
        out_shape=[
            jax.ShapeDtypeStruct((rows // 2, DH), F32),
            jax.ShapeDtypeStruct((peers, PLEN, DH), BF16),
        ],
        cost_estimate=cost(1 << 20, 1 << 20),
        name="finish",
    )(owners, own, left, right)


def collect_body(wanted_ref, returned_ref, out_ref):
    out_ref[...] = jnp.zeros_like(out_ref)
    for s in range(returned_ref.shape[0]):

        @pl.when(wanted_ref[s] >= 0)
        def _():
            at = jnp.maximum(wanted_ref[s], 0)
            out_ref[at] = out_ref[at] + returned_ref[s].astype(F32)


def collect(wanted, returned, passages):
    return pl.pallas_call(
        collect_body,
        in_specs=[SMEM, VMEM],
        out_specs=VMEM,
        out_shape=jax.ShapeDtypeStruct((passages, PLEN, DH), F32),
        cost_estimate=cost(1 << 20, 1 << 20),
        name="collect",
    )(wanted, returned)


def add_up_body(parts_ref, out_ref):
    out_ref[...] = jnp.sum(parts_ref[...].astype(F32), axis=0).T


def add_up(parts):
    return pl.pallas_call(
        add_up_body,
        in_specs=[VMEM],
        out_specs=VMEM,
        out_shape=jax.ShapeDtypeStruct(parts.shape[1:], F32),
        cost_estimate=cost(1 << 20, 1 << 20),
        name="add_up",
    )(parts)


def shards(normed, store, passage_ids, w_query, w_gate, w_key, w_value, cotangent):
    peers = lax.axis_size("st")
    members = lax.axis_size("tp")
    chips = members // 2
    pass_dev = store.shape[0] // PLEN
    flat_ids = passage_ids.reshape(-1)
    owners = flat_ids // pass_dev
    local_ids = flat_ids % pass_dev
    slot_hit = owners[:, None] == jnp.arange(peers, dtype=jnp.int32)[None, :]
    slot_table = jnp.max(jnp.where(slot_hit, local_ids[:, None], -1), axis=0)
    wanted = lax.all_to_all(slot_table.reshape(peers, 1), "st", 0, 0, tiled=True).reshape(peers)

    partner = [(t, t ^ 1) for t in range(members)]
    mine = (w_query, w_gate, w_key, w_value)
    theirs = tuple(lax.ppermute(w, "tp", partner) for w in mine)

    projected = project_rows(store, w_key, w_value, 256)
    served = serve(wanted, projected.reshape(pass_dev, PLEN, 2 * DH))
    arrived = lax.all_to_all(served, "st", 0, 0, tiled=True)
    queries, gate_open = project_tokens(normed, w_query, w_gate, 256)
    grads = attend(owners, queries, gate_open, cotangent, arrived)

    other = lax.ppermute(grads, "tp", partner)
    weight_parts = lax.all_to_all(weight_grad(grads, normed), "st", 0, 0, tiled=True)
    order = (4, 5, 3, 6, 2, 7, 1, 0)
    part = dict(zip(order, spread(order, chips, grads, other, mine + theirs)))

    def hop(array, by):
        return lax.ppermute(array, "tp", [(t, (t + 2 * by) % members) for t in range(members)])

    up = hop(part[4], 1)
    down = hop(part[5], -1)
    up = hop(part[3] + up, 1)
    down = hop(part[6] + down, -1)
    up = hop(part[2] + up, 1)
    down = hop(part[7] + down, -1)
    up = hop(part[1] + up, 1)
    grad_rows, outgoing = finish(owners, part[0], up, down, peers)
    returned = lax.all_to_all(outgoing, "st", 0, 0, tiled=True)
    grad_store = collect(wanted, returned, pass_dev).reshape(pass_dev * PLEN, DH)
    grad_query_weight = add_up(weight_parts)
    return (grad_rows, grad_store, grad_query_weight)


def solution(mesh):
    placed = (
        P("st", None),
        P("st", None),
        P("st", None),
        P(None, "tp"),
        P(None, "tp"),
        P(None, "tp"),
        P(None, "tp"),
        P("st", "tp"),
    )
    return jax.shard_map(
        shards,
        mesh=mesh,
        in_specs=placed,
        out_specs=(P("st", "tp"), P("st", "tp"), P("st", "tp")),
        check_vma=False,
    )
```

time: 171 us -> 118 us (0.69)
  waiting for transfers between devices: 70.1 us -> 31.9 us
  Pallas kernels: 0 us -> 33.2 us
  matrix products: 27.1 us -> 0 us
  local copies, waits for them, and re-layouts: 23.7 us -> 4.71 us
  starting transfers between devices: 26.8 us -> 40.7 us
  between operations: 14.2 us -> 0.8 us
    unnamed x2 -> x0, waiting for transfers between devices: 57.4 us -> none
    pallas_call x0 -> x9, Pallas kernels: none -> 33.2 us  [the longest x1 8.63 us: project_rows(): pl.pallas_call(project_body, grid=(rows // tile,), in_specs=[pl.BlockSpec...]
    dot_general x14 -> x0, matrix products: 25.1 us -> none  [the longest x1 6.8 us: shards(): jnp.dot(store, w_pair, preferred_element_type=jnp.float32)]
    ppermute x0 -> x12, waiting for transfers between devices: none -> 21 us  [the longest x7 18.9 us: hop(): lax.ppermute(array, 'tp', [(t, (t + 2 * by) % members) for t in range(mem...]
    ppermute x0 -> x12, starting transfers between devices: none -> 13.9 us  [the longest x7 12.8 us: hop(): lax.ppermute(array, 'tp', [(t, (t + 2 * by) % members) for t in range(mem...]
    unnamed x22 -> x25, local copies, waits for them, and re-layouts: 9.45 us -> 3.94 us
    add x1 -> x5, other arithmetic: 0.01 us -> 5.11 us  [the longest x1 1.03 us: shards(): down = hop(part[6] + down, -1)]
    gather x3 -> x0, local copies, waits for them, and re-layouts: 4.97 us -> none  [the longest x1 2.6 us: shards(): served = jnp.take(projected, jnp.maximum(served_ids, 0), axis=0)]
  transfers between devices with their start and end apart: 5 -> 16, of which waited for: 3 -> 7; matrix products, arithmetic and copies ran while one was open for 12% -> 4% of each run, Pallas kernels for 0% -> 20%
where the time goes in v1:
time: 118 us; the launch traced here: 117 us
  starting transfers between devices  40.7 us (34%)
  Pallas kernels  33.2 us (28%)
  waiting for transfers between devices  31.9 us (27%)
  other arithmetic  6.17 us (5%)
  local copies, waits for them, and re-layouts  4.71 us (4%)
    ppermute x7, waiting for transfers between devices, hop(): lax.ppermute(array, 'tp', [(t, (t + 2 * by) % members) for t in range(mem...  18.9 us
    ppermute x7, starting transfers between devices, hop(): lax.ppermute(array, 'tp', [(t, (t + 2 * by) % members) for t in range(mem...  12.8 us
    pallas_call x1, Pallas kernels, project_rows(): pl.pallas_call(project_body, grid=(rows // tile,), in_specs=[pl.BlockSpec...  8.63 us
    all_to_all x1, starting transfers between devices, shards(): lax.all_to_all(slot_table.reshape(peers, 1), 'st', 0, 0, tiled=True)  7.48 us
    all_to_all x1, starting transfers between devices, shards(): returned = lax.all_to_all(outgoing, 'st', 0, 0, tiled=True)  7.28 us
    all_to_all x1, starting transfers between devices, shards(): arrived = lax.all_to_all(served, 'st', 0, 0, tiled=True)  7.23 us
    pallas_call x1, Pallas kernels, spread(): pl.pallas_call(functools.partial(spread_body, steps, chips), in_specs=[VM...  5.53 us
    all_to_all x1, waiting for transfers between devices, shards(): returned = lax.all_to_all(outgoing, 'st', 0, 0, tiled=True)  5.51 us
  transfers between devices with their start and end apart: 16, of which 7 were waited for; matrix products, arithmetic and copies ran while one was open for 4% of the time, Pallas kernels for 20%

profile of v1, /device:TPU:2, one launch (start us, length us, event | category | flops | bytes accessed | tf_op | source)
XLA Modules:
  0.0 117.5 jit_solution(6668540919957609882)
XLA Ops:
  2.5 7.5 %all-to-all-start = ((s32[16,1,1]{2,1,0:T(1,128)}), s32[16,1,1]{2,1,0:T(1,128)S(1)}, u32[]{:S(2)}, u32[]{:S(2)}) async-start(s32[16,1,1]{2,1,0:T(1,128)} %copy.18), calls=%async_computation | async-start | bytes 16384 | tf_op jit(solution)/shard_map/all_to_all | solution.py:274
  9.9 8.6 %project_store.1 = bf16[2048,256]{1,0:T(8,128)(2,1)} custom-call(bf16[2048,2048]{1,0:T(8,128)(2,1)} %x_ref.4, bf16[2048,128]{1,0:T(8,128)(2,1)} %refs_2_.1, bf16[2048,128]{1,0:T(8,128)(2,1)} %refs_3_.1), custom_call_target="tpu_custom_call" | custom-call | flops 2147483648 | bytes 8388608 | tf_op jit(solution)/shard_map/project_store/pallas_call | solution.py:44
  19.5 2.1 %serve.1 = bf16[16,64,256]{2,1,0:T(8,128)(2,1)} custom-call(s32[16]{0:T(128)} %reduce.wanted_ref, bf16[32,64,256]{2,1,0:T(8,128)(2,1)} %bitcast.3), custom_call_target="tpu_custom_call" | custom-call | flops 1048576 | bytes 1048576 | tf_op jit(solution)/shard_map/serve/pallas_call | solution.py:95
  21.6 7.2 %all-to-all-start.1 = ((bf16[16,64,256]{2,1,0:T(8,128)(2,1)}), bf16[16,64,256]{2,1,0:T(8,128)(2,1)S(1)}, u32[]{:S(2)}, u32[]{:S(2)}) async-start(bf16[16,64,256]{2,1,0:T(8,128)(2,1)} %serve.1), calls=%async_computation.1 | async-start | bytes 1048576 | tf_op jit(solution)/shard_map/all_to_all | solution.py:282
  30.0 3.1 %project_tokens.1 = (bf16[512,128]{1,0:T(8,128)(2,1)}, f32[512,128]{1,0:T(8,128)}) custom-call(bf16[512,2048]{1,0:T(8,128)(2,1)} %x_ref.5, bf16[2048,128]{1,0:T(8,128)(2,1)} %refs_0_.1, bf16[2048,128]{1,0:T(8,128)(2,1)} %refs_1_.1), custom_call_target="tpu_custom_call" | custom-call | flops 536870912 | bytes 2097152 | tf_op jit(solution)/shard_map/project_tokens/pallas_call | solution.py:70
  33.1 5.4 %all-to-all-done.1.kv_ref = bf16[16,64,256]{2,1,0:T(8,128)(2,1)S(1)} async-done(((bf16[16,64,256]{2,1,0:T(8,128)(2,1)}), bf16[16,64,256]{2,1,0:T(8,128)(2,1)S(1)}, u32[]{:S(2)}, u32[]{:S(2)}) %all-to-all-start.1) | async-done | bytes 524320 | tf_op jit(solution)/shard_map/all_to_all | solution.py:282
  39.3 4.7 %attend.1.mine_ref.d_ref = bf16[1024,256]{1,0:T(8,128)(2,1)} custom-call(s32[8]{0:T(128)} %copy-done.11, bf16[512,128]{1,0:T(8,128)(2,1)} %get-tuple-element.15.q_ref, f32[512,128]{1,0:T(8,128)} %get-tuple-element.16.gate_ref, bf16[512,128]{1,0:T(8,128)(2,1)} %cot_ref.1, bf16[16,64,256]{2,1,0:T(8,128)(2,1)} %copy-done.5), custom_call_target="tpu_custom_call" | custom-call | flops 117440512 | bytes 1048576 | tf_op jit(solution)/shard_map/attend/pallas_call | solution.py:136
  44.0 2.1 %collective-permute-done.other_ref = bf16[1024,256]{1,0:T(8,128)(2,1)S(1)} collective-permute-done((bf16[1024,256]{1,0:T(8,128)(2,1)}, bf16[1024,256]{1,0:T(8,128)(2,1)S(1)}, u32[]{:S(2)}, u32[]{:S(2)}) %collective-permute-start) | collective-permute-done | bytes 524320 | tf_op jit(solution)/shard_map/ppermute | solution.py:286
  46.9 5.5 %spread_4_5_3_6_2_7_1_0.1 = (bf16[1024,128]{1,0:T(8,128)(2,1)}, bf16[1024,128]{1,0:T(8,128)(2,1)}, bf16[1024,128]{1,0:T(8,128)(2,1)}, bf16[1024,128]{1,0:T(8,128...) custom-call(bf16[1024,256]{1,0:T(8,128)(2,1)} %attend.1.mine_ref.d_r, ...), custom_call_target="tpu_custom_call" | custom-call | flops 1073741824 | bytes 4194304 | tf_op jit(solution)/shard_map/spread_4_5_3_6_2_7_1_0/pallas_call | solution.py:188
  52.4 1.9 %collective-permute-start.5 = (bf16[1024,128]{1,0:T(8,128)(2,1)}, bf16[1024,128]{1,0:T(8,128)(2,1)S(1)}, u32[]{:S(2)}, u32[]{:S(2)}) collective-permute-start(bf16[1024,128]{1,0:T(8,128)(2,1)} %get-tuple-element.21), channel_id=1, source_target_pairs={{0,2},{1,3},{2,4},{3,5},{4,6},{5,7},{6,8},{7,9},{8,10},{9,11},{10,... | collective-permute-start | bytes 786440 | tf_op jit(solution)/shard_map/ppermute | solution.py:292
  54.4 4.0 %collective-permute-start.9 = (bf16[1024,128]{1,0:T(8,128)(2,1)}, bf16[1024,128]{1,0:T(8,128)(2,1)S(1)}, u32[]{:S(2)}, u32[]{:S(2)}) collective-permute-start(bf16[1024,128]{1,0:T(8,128)(2,1)} %get-tuple-element.24), channel_id=1, source_target_pairs={{0,14},{1,15},{2,0},{3,1},{4,2},{5,3},{6,4},{7,5},{8,6},{9,7},{10,... | collective-permute-start | bytes 786440 | tf_op jit(solution)/shard_map/ppermute | solution.py:292
  58.4 6.7 %collective-permute-done.5 = bf16[1024,128]{1,0:T(8,128)(2,1)S(1)} collective-permute-done((bf16[1024,128]{1,0:T(8,128)(2,1)}, bf16[1024,128]{1,0:T(8,128)(2,1)S(1)}, u32[]{:S(2)}, u32[]{:S(2)}) %collective-permute-start.5) | collective-permute-done | bytes 262176 | tf_op jit(solution)/shard_map/ppermute | solution.py:292
  67.3 3.3 %collective-permute-start.10 = (bf16[1024,128]{1,0:T(8,128)(2,1)S(1)}, bf16[1024,128]{1,0:T(8,128)(2,1)S(1)}, u32[]{:S(2)}, u32[]{:S(2)}) collective-permute-start(bf16[1024,128]{1,0:T(8,128)(2,1)S(1)} %add.34), channel_id=1, source_target_pairs={{0,14},{1,15},{2,0},{3,1},{4,2},{5,3},{6,4},{7,5},{8,6},{9,7},{10,... | collective-permute-start | bytes 786440 | tf_op jit(solution)/shard_map/ppermute | solution.py:292
  70.6 4.6 %collective-permute-done.6 = bf16[1024,128]{1,0:T(8,128)(2,1)S(1)} collective-permute-done((bf16[1024,128]{1,0:T(8,128)(2,1)S(1)}, bf16[1024,128]{1,0:T(8,128)(2,1)S(1)}, u32[]{:S(2)}, u32[]{:S(2)}) %collective-permute-start.6) | collective-permute-done | bytes 262176 | tf_op jit(solution)/shard_map/ppermute | solution.py:292
  76.3 3.1 %weight_grad.1 = bf16[16,128,128]{2,1,0:T(8,128)(2,1)} custom-call(bf16[1024,256]{1,0:T(8,128)(2,1)} %attend.1.mine_ref.d_ref, bf16[512,2048]{1,0:T(8,128)(2,1)} %x_ref.5), custom_call_target="tpu_custom_call" | custom-call | flops 268435456 | bytes 2097152 | tf_op jit(solution)/shard_map/weight_grad/pallas_call | solution.py:157
  79.4 4.8 %all-to-all-start.3 = ((bf16[16,128,128]{2,1,0:T(8,128)(2,1)}), bf16[16,128,128]{2,1,0:T(8,128)(2,1)S(1)}, u32[]{:S(2)}, u32[]{:S(2)}) async-start(bf16[16,128,128]{2,1,0:T(8,128)(2,1)} %weight_grad.1), calls=%async_computation.3 | async-start | bytes 1048576 | tf_op jit(solution)/shard_map/all_to_all | solution.py:287
  85.2 3.3 %collective-permute-start.11 = (bf16[1024,128]{1,0:T(8,128)(2,1)S(1)}, bf16[1024,128]{1,0:T(8,128)(2,1)S(1)}, u32[]{:S(2)}, u32[]{:S(2)}) collective-permute-start(bf16[1024,128]{1,0:T(8,128)(2,1)S(1)} %add.35), channel_id=1, source_target_pairs={{0,14},{1,15},{2,0},{3,1},{4,2},{5,3},{6,4},{7,5},{8,6},{9,7},{10,... | collective-permute-start | bytes 786440 | tf_op jit(solution)/shard_map/ppermute | solution.py:292
  89.6 2.8 %collective-permute-done.11.right_ref = bf16[1024,128]{1,0:T(8,128)(2,1)S(1)} collective-permute-done((bf16[1024,128]{1,0:T(8,128)(2,1)S(1)}, bf16[1024,128]{1,0:T(8,128)(2,1)S(1)}, u32[]{:S(2)}, u32[]{:S(2)}) %collective-permute-start.11) | collective-permute-done | bytes 262176 | tf_op jit(solution)/shard_map/ppermute | solution.py:292
  92.4 4.8 %collective-permute-done.8.left_ref = bf16[1024,128]{1,0:T(8,128)(2,1)S(1)} collective-permute-done((bf16[1024,128]{1,0:T(8,128)(2,1)S(1)}, bf16[1024,128]{1,0:T(8,128)(2,1)S(1)}, u32[]{:S(2)}, u32[]{:S(2)}) %collective-permute-start.8) | collective-permute-done | bytes 262176 | tf_op jit(solution)/shard_map/ppermute | solution.py:292
  97.9 2.0 %finish.1 = (f32[512,128]{1,0:T(8,128)}, bf16[16,64,128]{2,1,0:T(8,128)(2,1)}) custom-call(s32[8]{0:T(128)} %copy-done.11, bf16[1024,128]{1,0:T(8,128)(2,1)} %get-tuple-element.17.own_ref, bf16[1024,128]{1,0:T(8,128)(2,1)} %copy-done.10, bf16[1024,128]{1,0:T(8,128)(2,1)} %copy-done.9), custom_call_target="tpu_custom_call" | custom-call | flops 1048576 | bytes 1048576 | tf_op jit(solution)/shard_map/finish/pallas_call | solution.py:215
  99.9 7.3 %all-to-all-start.2 = ((bf16[16,64,128]{2,1,0:T(8,128)(2,1)}), bf16[16,64,128]{2,1,0:T(8,128)(2,1)S(1)}, u32[]{:S(2)}, u32[]{:S(2)}) async-start(bf16[16,64,128]{2,1,0:T(8,128)(2,1)} %get-tuple-element.26), calls=%async_computation.2 | async-start | bytes 524288 | tf_op jit(solution)/shard_map/all_to_all | solution.py:302
  107.2 1.8 %add_up.1 = f32[128,128]{1,0:T(8,128)} custom-call(bf16[16,128,128]{2,1,0:T(8,128)(2,1)} %copy-done.4), custom_call_target="tpu_custom_call" | custom-call | flops 1048576 | bytes 1048576 | tf_op jit(solution)/shard_map/add_up/pallas_call | solution.py:254
  109.0 5.5 %all-to-all-done.2.returned_ref = bf16[16,64,128]{2,1,0:T(8,128)(2,1)S(1)} async-done(((bf16[16,64,128]{2,1,0:T(8,128)(2,1)}), bf16[16,64,128]{2,1,0:T(8,128)(2,1)S(1)}, u32[]{:S(2)}, u32[]{:S(2)}) %all-to-all-start.2) | async-done | bytes 262176 | tf_op jit(solution)/shard_map/all_to_all | solution.py:302
  115.3 2.2 %collect.1 = f32[32,64,128]{2,1,0:T(8,128)} custom-call(s32[16]{0:T(128)} %reduce.wanted_ref, bf16[16,64,128]{2,1,0:T(8,128)(2,1)} %copy-done.6), custom_call_target="tpu_custom_call" | custom-call | flops 1048576 | bytes 1048576 | tf_op jit(solution)/shard_map/collect/pallas_call | solution.py:239
  (52 shorter events, 12.2 us)
Async XLA Ops:
  0.6 28.2 %copy-start = (bf16[2048,128]{1,0:T(8,128)(2,1)S(1)}, bf16[2048,128]{1,0:T(8,128)(2,1)}, u32[]{:S(2)}) copy-start(bf16[2048,128]{1,0:T(8,128)(2,1)} %refs_2_.1) | copy-start | bytes 1572868
  0.6 28.3 %copy-start.1 = (bf16[2048,128]{1,0:T(8,128)(2,1)S(1)}, bf16[2048,128]{1,0:T(8,128)(2,1)}, u32[]{:S(2)}) copy-start(bf16[2048,128]{1,0:T(8,128)(2,1)} %refs_3_.1) | copy-start | bytes 1572868
  0.7 28.8 %copy-start.2 = (bf16[2048,128]{1,0:T(8,128)(2,1)S(1)}, bf16[2048,128]{1,0:T(8,128)(2,1)}, u32[]{:S(2)}) copy-start(bf16[2048,128]{1,0:T(8,128)(2,1)} %refs_0_.1) | copy-start | bytes 1572868
  0.7 28.9 %copy-start.3 = (bf16[2048,128]{1,0:T(8,128)(2,1)S(1)}, bf16[2048,128]{1,0:T(8,128)(2,1)}, u32[]{:S(2)}) copy-start(bf16[2048,128]{1,0:T(8,128)(2,1)} %refs_1_.1) | copy-start | bytes 1572868
  1.7 36.8 %copy-start.11 = (s32[8]{0:T(128)}, s32[8]{0:T(128)S(1)}, u32[]{:S(2)}) copy-start(s32[8]{0:T(128)S(1)} %get-tuple-element.28.owner_ref) | copy-start | bytes 100
  2.5 16.1 %all-to-all-start = ((s32[16,1,1]{2,1,0:T(1,128)}), s32[16,1,1]{2,1,0:T(1,128)S(1)}, u32[]{:S(2)}, u32[]{:S(2)}) async-start(s32[16,1,1]{2,1,0:T(1,128)} %copy.18), calls=%async_computation | async-start | bytes 16384 | tf_op jit(solution)/shard_map/all_to_all | solution.py:274
  21.6 16.8 %all-to-all-start.1 = ((bf16[16,64,256]{2,1,0:T(8,128)(2,1)}), bf16[16,64,256]{2,1,0:T(8,128)(2,1)S(1)}, u32[]{:S(2)}, u32[]{:S(2)}) async-start(bf16[16,64,256]{2,1,0:T(8,128)(2,1)} %serve.1), calls=%async_computation.1 | async-start | bytes 1048576 | tf_op jit(solution)/shard_map/all_to_all | solution.py:282
  28.9 15.1 %collective-permute-start.3 = (bf16[2048,128]{1,0:T(8,128)(2,1)S(1)}, bf16[2048,128]{1,0:T(8,128)(2,1)S(1)}, u32[]{:S(2)}, u32[]{:S(2)}) collective-permute-start(bf16[2048,128]{1,0:T(8,128)(2,1)S(1)} %copy-done), channel_id=1, source_target_pairs={{0,1},{1,0},{2,3},{3,2},{4,5},{5,4},{6,7},{7,6},{8,9},{9,8},{10,11... | collective-permute-start | bytes 1572872 | tf_op jit(solution)/shard_map/ppermute | solution.py:278
  29.0 15.1 %collective-permute-start.4 = (bf16[2048,128]{1,0:T(8,128)(2,1)S(1)}, bf16[2048,128]{1,0:T(8,128)(2,1)}, u32[]{:S(2)}, u32[]{:S(2)}) collective-permute-start(bf16[2048,128]{1,0:T(8,128)(2,1)S(1)} %copy-done.1), channel_id=1, source_target_pairs={{0,1},{1,0},{2,3},{3,2},{4,5},{5,4},{6,7},{7,6},{8,9},{9,8},{10,11... | collective-permute-start | bytes 1572872 | tf_op jit(solution)/shard_map/ppermute | solution.py:278
  29.5 14.5 %collective-permute-start.1 = (bf16[2048,128]{1,0:T(8,128)(2,1)S(1)}, bf16[2048,128]{1,0:T(8,128)(2,1)}, u32[]{:S(2)}, u32[]{:S(2)}) collective-permute-start(bf16[2048,128]{1,0:T(8,128)(2,1)S(1)} %copy-done.2), channel_id=1, source_target_pairs={{0,1},{1,0},{2,3},{3,2},{4,5},{5,4},{6,7},{7,6},{8,9},{9,8},{10,11... | collective-permute-start | bytes 1572872 | tf_op jit(solution)/shard_map/ppermute | solution.py:278
  29.6 14.4 %collective-permute-start.2 = (bf16[2048,128]{1,0:T(8,128)(2,1)S(1)}, bf16[2048,128]{1,0:T(8,128)(2,1)}, u32[]{:S(2)}, u32[]{:S(2)}) collective-permute-start(bf16[2048,128]{1,0:T(8,128)(2,1)S(1)} %copy-done.3), channel_id=1, source_target_pairs={{0,1},{1,0},{2,3},{3,2},{4,5},{5,4},{6,7},{7,6},{8,9},{9,8},{10,11... | collective-permute-start | bytes 1572872 | tf_op jit(solution)/shard_map/ppermute | solution.py:278
  44.0 2.1 %collective-permute-start = (bf16[1024,256]{1,0:T(8,128)(2,1)}, bf16[1024,256]{1,0:T(8,128)(2,1)S(1)}, u32[]{:S(2)}, u32[]{:S(2)}) collective-permute-start(bf16[1024,256]{1,0:T(8,128)(2,1)} %attend.1.mine_ref.d_ref), channel_id=1, source_target_pairs={{0,1},{1,0},{2,3},{3,2},{4,5},{5,4},{6,7},{7,6},{8,9},{9,8},{10,11... | collective-permute-start | bytes 1572872 | tf_op jit(solution)/shard_map/ppermute | solution.py:286
  44.0 2.1 %copy-start.7 = (bf16[2048,128]{1,0:T(8,128)(2,1)}, bf16[2048,128]{1,0:T(8,128)(2,1)S(1)}, u32[]{:S(2)}) copy-start(bf16[2048,128]{1,0:T(8,128)(2,1)S(1)} %collective-permute-done.3.refs_6_) | copy-start | bytes 1572868
  52.4 12.7 %collective-permute-start.5 = (bf16[1024,128]{1,0:T(8,128)(2,1)}, bf16[1024,128]{1,0:T(8,128)(2,1)S(1)}, u32[]{:S(2)}, u32[]{:S(2)}) collective-permute-start(bf16[1024,128]{1,0:T(8,128)(2,1)} %get-tuple-element.21), channel_id=1, source_target_pairs={{0,2},{1,3},{2,4},{3,5},{4,6},{5,7},{6,8},{7,9},{8,10},{9,11},{10,... | collective-permute-start | bytes 786440 | tf_op jit(solution)/shard_map/ppermute | solution.py:292
  54.4 11.9 %collective-permute-start.9 = (bf16[1024,128]{1,0:T(8,128)(2,1)}, bf16[1024,128]{1,0:T(8,128)(2,1)S(1)}, u32[]{:S(2)}, u32[]{:S(2)}) collective-permute-start(bf16[1024,128]{1,0:T(8,128)(2,1)} %get-tuple-element.24), channel_id=1, source_target_pairs={{0,14},{1,15},{2,0},{3,1},{4,2},{5,3},{6,4},{7,5},{8,6},{9,7},{10,... | collective-permute-start | bytes 786440 | tf_op jit(solution)/shard_map/ppermute | solution.py:292
  66.1 9.1 %collective-permute-start.6 = (bf16[1024,128]{1,0:T(8,128)(2,1)S(1)}, bf16[1024,128]{1,0:T(8,128)(2,1)S(1)}, u32[]{:S(2)}, u32[]{:S(2)}) collective-permute-start(bf16[1024,128]{1,0:T(8,128)(2,1)S(1)} %add.31), channel_id=1, source_target_pairs={{0,2},{1,3},{2,4},{3,5},{4,6},{5,7},{6,8},{7,9},{8,10},{9,11},{10,... | collective-permute-start | bytes 786440 | tf_op jit(solution)/shard_map/ppermute | solution.py:292
  67.3 16.9 %collective-permute-start.10 = (bf16[1024,128]{1,0:T(8,128)(2,1)S(1)}, bf16[1024,128]{1,0:T(8,128)(2,1)S(1)}, u32[]{:S(2)}, u32[]{:S(2)}) collective-permute-start(bf16[1024,128]{1,0:T(8,128)(2,1)S(1)} %add.34), channel_id=1, source_target_pairs={{0,14},{1,15},{2,0},{3,1},{4,2},{5,3},{6,4},{7,5},{8,6},{9,7},{10,... | collective-permute-start | bytes 786440 | tf_op jit(solution)/shard_map/ppermute | solution.py:292
  76.2 12.3 %collective-permute-start.7 = (bf16[1024,128]{1,0:T(8,128)(2,1)S(1)}, bf16[1024,128]{1,0:T(8,128)(2,1)S(1)}, u32[]{:S(2)}, u32[]{:S(2)}) collective-permute-start(bf16[1024,128]{1,0:T(8,128)(2,1)S(1)} %add.32), channel_id=1, source_target_pairs={{0,2},{1,3},{2,4},{3,5},{4,6},{5,7},{6,8},{7,9},{8,10},{9,11},{10,... | collective-permute-start | bytes 786440 | tf_op jit(solution)/shard_map/ppermute | solution.py:292
  79.4 20.6 %all-to-all-start.3 = ((bf16[16,128,128]{2,1,0:T(8,128)(2,1)}), bf16[16,128,128]{2,1,0:T(8,128)(2,1)S(1)}, u32[]{:S(2)}, u32[]{:S(2)}) async-start(bf16[16,128,128]{2,1,0:T(8,128)(2,1)} %weight_grad.1), calls=%async_computation.3 | async-start | bytes 1048576 | tf_op jit(solution)/shard_map/all_to_all | solution.py:287
  85.2 7.2 %collective-permute-start.11 = (bf16[1024,128]{1,0:T(8,128)(2,1)S(1)}, bf16[1024,128]{1,0:T(8,128)(2,1)S(1)}, u32[]{:S(2)}, u32[]{:S(2)}) collective-permute-start(bf16[1024,128]{1,0:T(8,128)(2,1)S(1)} %add.35), channel_id=1, source_target_pairs={{0,14},{1,15},{2,0},{3,1},{4,2},{5,3},{6,4},{7,5},{8,6},{9,7},{10,... | collective-permute-start | bytes 786440 | tf_op jit(solution)/shard_map/ppermute | solution.py:292
  89.5 7.7 %collective-permute-start.8 = (bf16[1024,128]{1,0:T(8,128)(2,1)S(1)}, bf16[1024,128]{1,0:T(8,128)(2,1)S(1)}, u32[]{:S(2)}, u32[]{:S(2)}) collective-permute-start(bf16[1024,128]{1,0:T(8,128)(2,1)S(1)} %add.33), channel_id=1, source_target_pairs={{0,2},{1,3},{2,4},{3,5},{4,6},{5,7},{6,8},{7,9},{8,10},{9,11},{10,... | collective-permute-start | bytes 786440 | tf_op jit(solution)/shard_map/ppermute | solution.py:292
  92.4 4.8 %copy-start.9 = (bf16[1024,128]{1,0:T(8,128)(2,1)}, bf16[1024,128]{1,0:T(8,128)(2,1)S(1)}, u32[]{:S(2)}) copy-start(bf16[1024,128]{1,0:T(8,128)(2,1)S(1)} %collective-permute-done.11.right_ref) | copy-start | bytes 786436
  99.9 7.3 %copy-start.4 = (bf16[16,128,128]{2,1,0:T(8,128)(2,1)}, bf16[16,128,128]{2,1,0:T(8,128)(2,1)S(1)}, u32[]{:S(2)}) copy-start(bf16[16,128,128]{2,1,0:T(8,128)(2,1)S(1)} %all-to-all-done.3.parts_ref) | copy-start | bytes 1572868
  99.9 14.6 %all-to-all-start.2 = ((bf16[16,64,128]{2,1,0:T(8,128)(2,1)}), bf16[16,64,128]{2,1,0:T(8,128)(2,1)S(1)}, u32[]{:S(2)}, u32[]{:S(2)}) async-start(bf16[16,64,128]{2,1,0:T(8,128)(2,1)} %get-tuple-element.26), calls=%async_computation.2 | async-start | bytes 524288 | tf_op jit(solution)/shard_map/all_to_all | solution.py:302
  (4 other events, 3.0 us)

commit v2 on v1

v2 whole, which is shorter than its diff:
```python
import functools

import jax
import jax.numpy as jnp
from jax import lax
from jax.experimental import pallas as pl
from jax.experimental.pallas import tpu as pltpu
from jax.sharding import PartitionSpec as P


DH = 128
BLK = 128
PLEN = 64
BF16 = jnp.bfloat16
F32 = jnp.float32
NEAR = 40
TOKENS = 40
ATTEND = 8
SERVE = 61
GRAD = 40

VMEM = pl.BlockSpec(memory_space=pltpu.VMEM)
SMEM = pl.BlockSpec(memory_space=pltpu.SMEM)


def nt(a, b):
    return lax.dot_general(a, b, (((1,), (1,)), ((), ())), preferred_element_type=F32)


def tn(a, b):
    return lax.dot_general(a, b, (((0,), (0,)), ((), ())), preferred_element_type=F32)


def nn(a, b):
    return lax.dot_general(a, b, (((1,), (0,)), ((), ())), preferred_element_type=F32)


def grant(mib):
    return pltpu.CompilerParams(vmem_limit_bytes=mib << 20)


def cost(flops, nbytes):
    return pl.CostEstimate(flops=flops, bytes_accessed=nbytes, transcendentals=0)


def request_body(pass_dev, ids_ref, table_ref, owner_ref):
    reads, blocks = ids_ref.shape
    lanes = table_ref.shape[1:]
    table_ref[...] = jnp.full(table_ref.shape, -1, jnp.int32)
    for b in range(blocks):
        for r in range(reads):
            passage = ids_ref[r, b]
            owner = lax.div(passage, pass_dev)
            table_ref[owner] = jnp.full(lanes, passage - owner * pass_dev, jnp.int32)
            owner_ref[b * reads + r] = owner


def request(passage_ids, pass_dev, peers):
    return pl.pallas_call(
        functools.partial(request_body, pass_dev),
        in_specs=[SMEM],
        out_specs=[VMEM, SMEM],
        out_shape=[
            jax.ShapeDtypeStruct((peers, 1, 128), jnp.int32),
            jax.ShapeDtypeStruct((passage_ids.size,), jnp.int32),
        ],
        cost_estimate=cost(1 << 16, 1 << 16),
        name="request",
    )(passage_ids.T)


def project_body(x_ref, wa_ref, wb_ref, out_ref):
    pair = jnp.concatenate([wa_ref[...], wb_ref[...]], axis=1)
    out_ref[...] = nn(x_ref[...], pair).astype(BF16)


def project_rows(store, w_key, w_value, tile):
    rows, width = store.shape
    cols = w_key.shape[1]
    return pl.pallas_call(
        project_body,
        grid=(rows // tile,),
        in_specs=[
            pl.BlockSpec((tile, width), lambda i: (i, 0)),
            pl.BlockSpec((width, cols), lambda i: (0, 0)),
            pl.BlockSpec((width, cols), lambda i: (0, 0)),
        ],
        out_specs=pl.BlockSpec((tile, 2 * cols), lambda i: (i, 0)),
        out_shape=jax.ShapeDtypeStruct((rows, 2 * cols), BF16),
        cost_estimate=cost(4 * rows * width * cols, 2 * rows * width),
        name="project_store",
    )(store, w_key, w_value)


def serve_body(wanted_ref, rows_ref, out_ref, kept_ref):
    last = rows_ref.shape[0] - 1
    for s in range(out_ref.shape[0]):
        kept_ref[s] = wanted_ref[s, 0, 0]
        out_ref[s] = rows_ref[jnp.clip(wanted_ref[s, 0, 0], 0, last)]


def serve(wanted, projected):
    peers = wanted.shape[0]
    return pl.pallas_call(
        serve_body,
        in_specs=[SMEM, VMEM],
        out_specs=[VMEM, SMEM],
        out_shape=[
            jax.ShapeDtypeStruct((peers,) + projected.shape[1:], BF16),
            jax.ShapeDtypeStruct((peers,), jnp.int32),
        ],
        compiler_params=grant(SERVE),
        cost_estimate=cost(1 << 20, 2 << 20),
        name="serve",
    )(wanted, projected)


def query_body(x_ref, wa_ref, wb_ref, cot_ref, q_ref, up_ref, slope_ref):
    cols = wa_ref.shape[1]
    pair = jnp.concatenate([wa_ref[...], wb_ref[...]], axis=1)
    both = nn(x_ref[...], pair)
    q_ref[...] = both[:, :cols].astype(BF16)
    gate = jax.nn.sigmoid(both[:, cols:])
    up = cot_ref[...].astype(F32) * gate
    up_ref[...] = up.astype(BF16)
    slope_ref[...] = (up * (1.0 - gate)).astype(BF16)


def project_tokens(normed, w_query, w_gate, cotangent, tile):
    rows, width = normed.shape
    cols = w_query.shape[1]
    return pl.pallas_call(
        query_body,
        grid=(rows // tile,),
        in_specs=[
            pl.BlockSpec((tile, width), lambda i: (i, 0)),
            pl.BlockSpec((width, cols), lambda i: (0, 0)),
            pl.BlockSpec((width, cols), lambda i: (0, 0)),
            pl.BlockSpec((tile, cols), lambda i: (i, 0)),
        ],
        out_specs=[pl.BlockSpec((tile, cols), lambda i: (i, 0))] * 3,
        out_shape=[jax.ShapeDtypeStruct((rows, cols), BF16)] * 3,
        compiler_params=grant(TOKENS),
        cost_estimate=cost(4 * rows * width * cols, 2 * rows * width),
        name="project_tokens",
    )(normed, w_query, w_gate, cotangent)


def attend_body(owner_ref, q_ref, up_ref, slope_ref, kv_ref, out_ref):
    scale = DH ** (-0.5)
    tokens = q_ref.shape[0]
    reads = BLK // PLEN
    blocks = range(tokens // BLK)
    rows = [slice(b * BLK, (b + 1) * BLK) for b in blocks]
    kv = [
        jnp.concatenate([kv_ref[owner_ref[reads * b + r]] for r in range(reads)], axis=0)
        for b in blocks
    ]
    scores = [nt(q_ref[rows[b], :], kv[b][:, :DH]) * scale for b in blocks]
    d_att = [up_ref[rows[b], :] for b in blocks]
    d_probs = [nt(d_att[b], kv[b][:, DH:]) for b in blocks]
    grown = [jnp.exp(x - jnp.max(x, axis=1, keepdims=True)) for x in scores]
    probs = [x / jnp.sum(x, axis=1, keepdims=True) for x in grown]
    low = [x.astype(BF16) for x in probs]
    attended = [nn(low[b], kv[b][:, DH:]) for b in blocks]
    delta = [jnp.sum(d_probs[b] * probs[b], axis=1, keepdims=True) for b in blocks]
    d_scores = [(probs[b] * (d_probs[b] - delta[b]) * scale).astype(BF16) for b in blocks]
    for b in blocks:
        at = slice(tokens + b * BLK, tokens + (b + 1) * BLK)
        out_ref[at, DH:] = tn(low[b], d_att[b]).astype(BF16)
    for b in blocks:
        out_ref[rows[b], :DH] = nn(d_scores[b], kv[b][:, :DH]).astype(BF16)
    for b in blocks:
        out_ref[rows[b], DH:] = (slope_ref[rows[b], :].astype(F32) * attended[b]).astype(BF16)
    for b in blocks:
        at = slice(tokens + b * BLK, tokens + (b + 1) * BLK)
        out_ref[at, :DH] = tn(d_scores[b], q_ref[rows[b], :]).astype(BF16)


def attend(owners, queries, upstream, slope, arrived):
    tokens = queries.shape[0]
    return pl.pallas_call(
        attend_body,
        in_specs=[SMEM, VMEM, VMEM, VMEM, VMEM],
        out_specs=VMEM,
        out_shape=jax.ShapeDtypeStruct((2 * tokens, 2 * DH), BF16),
        cost_estimate=cost(14 * tokens * DH * DH, 1 << 20),
        compiler_params=grant(ATTEND),
        name="attend",
    )(owners, queries, upstream, slope, arrived)


def weight_grad_body(d_ref, x_ref, out_ref):
    d_query = d_ref[: x_ref.shape[0], :DH]
    flipped = d_query.astype(F32).T.astype(BF16)
    for j in range(out_ref.shape[0] // 2):
        both = nn(flipped, x_ref[:, 2 * j * DH : 2 * (j + 1) * DH]).astype(BF16)
        out_ref[2 * j] = both[:, :DH]
        out_ref[2 * j + 1] = both[:, DH:]


def weight_grad(grads, normed):
    tokens, width = normed.shape
    return pl.pallas_call(
        weight_grad_body,
        in_specs=[VMEM, VMEM],
        out_specs=VMEM,
        out_shape=jax.ShapeDtypeStruct((width // DH, DH, DH), BF16),
        compiler_params=grant(GRAD),
        cost_estimate=cost(2 * tokens * width * DH, 2 * tokens * width),
        name="weight_grad",
    )(grads, normed)


def both_heads(mine_ref, other_ref, side):
    return jnp.concatenate([mine_ref[side, :], other_ref[side, :]], axis=1)


def place(chips):
    at = lax.axis_index("tp")
    core = lax.rem(at, 2)
    chip = lax.div(at, 2)

    def first_row(k):
        to = lax.rem(chip + k + core * (chips - 2 * k), chips)
        return pl.multiple_of(to * 2 * DH, 2 * DH)

    return core, chip, first_row


JOBS = ((1, 3), (0, 3), (1, 2), (0, 2), (1, 1), (0, 1), (1, 0), (0, 0))


def pick_body(chips, *refs):
    weights, (far_ref, near_ref, far_sems, near_sems) = refs[:8], refs[8:]
    core, chip, first_row = place(chips)

    def source(half, piece):
        return weights[(2 * half, 2 * half + 1, 4 + 2 * half, 5 + 2 * half)[piece]]

    def far_copy(half, piece):
        return pltpu.make_async_copy(
            source(half, piece).at[pl.ds(first_row(chips // 2), 2 * DH), :],
            far_ref.at[:, pl.ds(piece * DH, DH)],
            far_sems.at[piece],
        )

    def near_copy(job, piece):
        half, k = JOBS[job]
        start = first_row(k) if k else pl.multiple_of((2 * chip + core) * DH, DH)
        count = 2 * DH if k else DH
        return pltpu.make_async_copy(
            source(half, piece).at[pl.ds(start, count), :],
            near_ref.at[job, pl.ds(0, count), pl.ds(piece * DH, DH)],
            near_sems.at[job, piece],
        )

    for half in range(2):

        @pl.when(core == half)
        def _():
            for piece in range(4):
                far_copy(half, piece).start()

    pairs = [(job, piece) for job in range(len(JOBS)) for piece in range(4)]
    for job, piece in pairs:
        near_copy(job, piece).start()
    for piece in range(4):
        far_copy(0, piece).wait()
    for job, piece in pairs:
        near_copy(job, piece).wait()


def pick(chips, weights):
    return pl.pallas_call(
        functools.partial(pick_body, chips),
        in_specs=[pl.BlockSpec(memory_space=pltpu.HBM)] * 8,
        out_specs=[VMEM] * 2,
        out_shape=[
            jax.ShapeDtypeStruct((2 * DH, 4 * DH), BF16),
            jax.ShapeDtypeStruct((len(JOBS), 2 * DH, 4 * DH), BF16),
        ],
        scratch_shapes=[pltpu.SemaphoreType.DMA((4,)), pltpu.SemaphoreType.DMA((len(JOBS), 4))],
        cost_estimate=cost(1 << 28, 6 << 20),
        name="pick",
    )(*weights)


def far_body(mine_ref, other_ref, weight_ref, out_ref):
    core = lax.rem(lax.axis_index("tp"), 2)
    tokens = out_ref.shape[0]
    side = pl.ds(pl.multiple_of(core * tokens, tokens), tokens)
    out_ref[...] = nt(both_heads(mine_ref, other_ref, side), weight_ref[...]).astype(BF16)


def far(mine, other, weight):
    tokens = mine.shape[0] // 2
    return pl.pallas_call(
        far_body,
        in_specs=[VMEM] * 3,
        out_specs=VMEM,
        out_shape=jax.ShapeDtypeStruct((tokens, 2 * DH), BF16),
        compiler_params=grant(8),
        cost_estimate=cost(16 * tokens * DH * DH, 1 << 20),
        name="far",
    )(mine, other, weight)


def near_body(mine_ref, other_ref, held_ref, *outs):
    tokens = mine_ref.shape[0] // 2
    left = [both_heads(mine_ref, other_ref, slice(h * tokens, (h + 1) * tokens)) for h in range(2)]
    for job, (half, k) in enumerate(JOBS):
        right = held_ref[job, : 2 * DH if k else DH, :]
        outs[job][...] = nt(left[half], right).astype(BF16)


def near(mine, other, held):
    tokens = mine.shape[0] // 2
    return pl.pallas_call(
        near_body,
        in_specs=[VMEM] * 3,
        out_specs=[VMEM] * len(JOBS),
        out_shape=[
            jax.ShapeDtypeStruct((tokens, 2 * DH if k else DH), BF16) for _, k in JOBS
        ],
        compiler_params=grant(NEAR),
        cost_estimate=cost(56 * 2 * tokens * DH * DH, 4 << 20),
        name="near",
    )(mine, other, held)


def join_body(chosen, own_ref, came_ref, out_ref):
    came = came_ref[...].astype(F32)
    if chosen is not None:
        core = lax.rem(lax.axis_index("tp"), 2)
        came = jnp.where(core == chosen, came, jnp.zeros_like(came))
    out_ref[...] = (own_ref[...].astype(F32) + came).astype(BF16)


def join(own, came, chosen=None):
    return pl.pallas_call(
        functools.partial(join_body, chosen),
        in_specs=[VMEM] * 2,
        out_specs=VMEM,
        out_shape=jax.ShapeDtypeStruct(own.shape, BF16),
        compiler_params=grant(4),
        cost_estimate=cost(1 << 20, 1 << 20),
    )(own, came)


def part_body(own_ref, came_ref, same_ref, cross_ref):
    both = own_ref[...].astype(F32) + came_ref[...].astype(F32)
    core = lax.rem(lax.axis_index("tp"), 2)
    same_ref[...] = jnp.where(core == 0, both[:, :DH], both[:, DH:]).astype(BF16)
    cross_ref[...] = jnp.where(core == 0, both[:, DH:], both[:, :DH]).astype(BF16)


def part(own, came):
    return pl.pallas_call(
        part_body,
        in_specs=[VMEM] * 2,
        out_specs=[VMEM] * 2,
        out_shape=[jax.ShapeDtypeStruct((own.shape[0], DH), BF16)] * 2,
        compiler_params=grant(4),
        cost_estimate=cost(1 << 20, 1 << 20),
    )(own, came)


def total(own_ref, ours_ref, theirs_ref, at):
    return own_ref[at, :].astype(F32) + ours_ref[at, :].astype(F32) + theirs_ref[at, :].astype(F32)


def finish_reads_body(owner_ref, own_ref, ours_ref, theirs_ref, slots_ref):
    slots_ref[...] = jnp.zeros_like(slots_ref)
    for i in range(own_ref.shape[0] // PLEN):
        at = slice(i * PLEN, (i + 1) * PLEN)
        slots_ref[owner_ref[i]] = total(own_ref, ours_ref, theirs_ref, at).astype(BF16)


def finish_reads(owners, own, ours, theirs, peers):
    return pl.pallas_call(
        finish_reads_body,
        in_specs=[SMEM, VMEM, VMEM, VMEM],
        out_specs=VMEM,
        out_shape=jax.ShapeDtypeStruct((peers, PLEN, DH), BF16),
        compiler_params=grant(8),
        cost_estimate=cost(1 << 20, 1 << 20),
        name="finish_reads",
    )(owners, own, ours, theirs)


def finish_rows_body(own_ref, ours_ref, theirs_ref, out_ref):
    out_ref[...] = total(own_ref, ours_ref, theirs_ref, slice(0, own_ref.shape[0]))


def finish_rows(own, ours, theirs):
    return pl.pallas_call(
        finish_rows_body,
        in_specs=[VMEM] * 3,
        out_specs=VMEM,
        out_shape=jax.ShapeDtypeStruct(own.shape, F32),
        compiler_params=grant(8),
        cost_estimate=cost(1 << 20, 1 << 20),
        name="finish_rows",
    )(own, ours, theirs)


def collect_body(wanted_ref, returned_ref, out_ref, sum_ref, sems):
    pieces = sems.shape[0]
    count = out_ref.shape[0] // pieces

    def leave(i):
        at = pl.ds(i * count, count)
        return pltpu.make_async_copy(sum_ref.at[at], out_ref.at[at], sems.at[i])

    for i in range(pieces):
        sum_ref[i * count : (i + 1) * count] = jnp.zeros((count,) + sum_ref.shape[1:], F32)
        for s in range(returned_ref.shape[0]):
            passage = wanted_ref[s]

            @pl.when((passage >= i * count) & (passage < (i + 1) * count))
            def _():
                at = jnp.clip(passage, i * count, (i + 1) * count - 1)
                sum_ref[at] = sum_ref[at] + returned_ref[s].astype(F32)

        leave(i).start()
    for i in range(pieces):
        leave(i).wait()


def collect(wanted, returned, passages):
    pieces = 4
    return pl.pallas_call(
        collect_body,
        in_specs=[SMEM, VMEM],
        out_specs=pl.BlockSpec(memory_space=pltpu.HBM),
        out_shape=jax.ShapeDtypeStruct((passages, PLEN, DH), F32),
        scratch_shapes=[pltpu.VMEM((passages, PLEN, DH), F32), pltpu.SemaphoreType.DMA((pieces,))],
        compiler_params=grant(8),
        cost_estimate=cost(1 << 20, 1 << 20),
        name="collect",
    )(wanted, returned)


def add_up_body(parts_ref, out_ref):
    out_ref[...] = jnp.sum(parts_ref[...].astype(F32), axis=0).T


def add_up(parts):
    return pl.pallas_call(
        add_up_body,
        in_specs=[VMEM],
        out_specs=VMEM,
        out_shape=jax.ShapeDtypeStruct(parts.shape[1:], F32),
        cost_estimate=cost(1 << 20, 1 << 20),
        compiler_params=grant(4),
        name="add_up",
    )(parts)


def shards(normed, store, passage_ids, w_query, w_gate, w_key, w_value, cotangent):
    peers = lax.axis_size("st")
    members = lax.axis_size("tp")
    chips = members // 2
    pass_dev = store.shape[0] // PLEN
    table, owners = request(passage_ids, pass_dev, peers)
    wanted = lax.all_to_all(table, "st", 0, 0, tiled=True)

    partner = [(t, t ^ 1) for t in range(members)]
    along = [(2 * z + c, 2 * ((z + 1 - 2 * c) % chips) + c) for z in range(chips) for c in range(2)]
    across = [(a, b ^ 1) for a, b in along]

    def move(array, pairs):
        return lax.ppermute(array, "tp", pairs)

    mine = (w_query, w_gate, w_key, w_value)
    weights = mine + tuple(move(w, partner) for w in mine)
    projected = project_rows(store, w_key, w_value, 1024).reshape(pass_dev, PLEN, 2 * DH)
    wanted, weights, projected = lax.optimization_barrier((wanted, weights, projected))
    served, wanted = serve(wanted, projected)
    served, later, normed_later = lax.optimization_barrier((served, weights, normed))
    arrived = lax.all_to_all(served, "st", 0, 0, tiled=True)
    queries, upstream, slope = project_tokens(normed_later, later[0], later[1], cotangent, 256)
    weight4, held = pick(chips, later)
    arrived, weight4 = lax.optimization_barrier((arrived, weight4))
    grads = attend(owners, queries, upstream, slope, arrived)

    other = move(grads, partner)
    opposite = move(far(grads, other, weight4), along)
    reads3, rows3, reads2, rows2, reads1, rows1, reads0, rows0 = near(grads, other, held)
    reads = move(join(reads3, opposite, 1), along)
    parts = weight_grad(grads, normed)
    parts = lax.all_to_all(parts, "st", 0, 0, tiled=True)
    rows = move(join(rows3, opposite, 0), along)
    reads = move(join(reads2, reads), along)
    rows = move(join(rows2, rows), along)
    same, cross = part(reads1, reads)
    outgoing = finish_reads(owners, reads0, move(same, along), move(cross, across), peers)
    same, cross = part(rows1, rows)
    grad_rows = finish_rows(rows0, move(same, along), move(cross, across))
    returned = lax.all_to_all(outgoing, "st", 0, 0, tiled=True)
    grad_store = collect(wanted, returned, pass_dev).reshape(pass_dev * PLEN, DH)
    grad_query_weight = add_up(parts)
    return (grad_rows, grad_store, grad_query_weight)


def solution(mesh):
    placed = (
        P("st", None),
        P("st", None),
        P("st", None),
        P(None, "tp"),
        P(None, "tp"),
        P(None, "tp"),
        P(None, "tp"),
        P("st", "tp"),
    )
    return jax.shard_map(
        shards,
        mesh=mesh,
        in_specs=placed,
        out_specs=(P("st", "tp"), P("st", "tp"), P("st", "tp")),
        check_vma=False,
    )
```

time: 118 us -> 99.1 us (0.84)
  the two profiles are of different devices: /device:TPU:2 before, /device:TPU:1 now
where the time goes in v2:
time: 99.1 us; the launch traced here: 98.5 us
  starting transfers between devices  45.7 us (46%)
  Pallas kernels  23.8 us (24%)
  waiting for transfers between devices  21.5 us (22%)
  local copies, waits for them, and re-layouts  6.33 us (6%)
  between operations  1.08 us (1%)
    ppermute x14, starting transfers between devices, move(): return lax.ppermute(array, 'tp', pairs)  23.9 us
    ppermute x14, waiting for transfers between devices, move(): return lax.ppermute(array, 'tp', pairs)  16.5 us
    all_to_all x1, starting transfers between devices, shards(): returned = lax.all_to_all(outgoing, 'st', 0, 0, tiled=True)  6.87 us
    unnamed x42, local copies, waits for them, and re-layouts  6.33 us
    all_to_all x1, starting transfers between devices, shards(): arrived = lax.all_to_all(served, 'st', 0, 0, tiled=True)  6.15 us
    pallas_call x1, Pallas kernels, project_rows(): pl.pallas_call(project_body, grid=(rows // tile,), in_specs=[pl.BlockSpec...  5.85 us
    all_to_all x1, starting transfers between devices, shards(): wanted = lax.all_to_all(table, 'st', 0, 0, tiled=True)  5.06 us
    all_to_all x1, starting transfers between devices, shards(): parts = lax.all_to_all(parts, 'st', 0, 0, tiled=True)  3.71 us
  transfers between devices with their start and end apart: 18, of which 11 were waited for; matrix products, arithmetic and copies ran while one was open for 0% of the time, Pallas kernels for 18%

profile of v2, /device:TPU:1, one launch (start us, length us, event | category | flops | bytes accessed | tf_op | source)
XLA Modules:
  0.0 98.5 jit_solution(555100264131529132)
XLA Ops:
  0.6 3.3 %collective-permute-start = (bf16[2048,128]{1,0:T(8,128)(2,1)}, bf16[2048,128]{1,0:T(8,128)(2,1)}, u32[]{:S(2)}, u32[]{:S(2)}) collective-permute-start(bf16[2048,128]{1,0:T(8,128)(2,1)} %refs_0_), channel_id=1, source_target_pairs={{0,1},{1,0},{2,3},{3,2},{4,5},{5,4},{6,7},{7,6},{8,9},{9,8},{10,11... | collective-permute-start | bytes 1572872 | tf_op jit(solution)/shard_map/ppermute | solution.py:474
  5.9 5.1 %all-to-all-start = ((s32[16,1,128]{2,1,0:T(1,128)}), s32[16,1,128]{2,1,0:T(1,128)S(1)}, u32[]{:S(2)}, u32[]{:S(2)}) async-start(s32[16,1,128]{2,1,0:T(1,128)} %get-tuple-element.47), calls=%async_computation | async-start | bytes 16384 | tf_op jit(solution)/shard_map/all_to_all | solution.py:467
  10.9 5.8 %project_store.1 = bf16[2048,256]{1,0:T(8,128)(2,1)} custom-call(bf16[2048,2048]{1,0:T(8,128)(2,1)} %x_ref.2, bf16[2048,128]{1,0:T(8,128)(2,1)} %refs_2_, bf16[2048,128]{1,0:T(8,128)(2,1)} %refs_3_), custom_call_target="tpu_custom_call" | custom-call | flops 2147483648 | bytes 8388608 | tf_op jit(solution)/shard_map/project_store/pallas_call | solution.py:80
  17.9 2.1 %serve.1 = (bf16[16,64,256]{2,1,0:T(8,128)(2,1)}, s32[16]{0:T(128)}) custom-call(s32[16,1,128]{2,1,0:T(1,128)} %copy-done.20, bf16[32,64,256]{2,1,0:T(8,128)(2,1)} %bitcast.3), custom_call_target="tpu_custom_call" | custom-call | flops 1048576 | bytes 2097152 | tf_op jit(solution)/shard_map/serve/pallas_call | solution.py:104
  20.0 6.2 %all-to-all-start.1 = ((bf16[16,64,256]{2,1,0:T(8,128)(2,1)}), bf16[16,64,256]{2,1,0:T(8,128)(2,1)S(1)}, u32[]{:S(2)}, u32[]{:S(2)}) async-start(bf16[16,64,256]{2,1,0:T(8,128)(2,1)} %get-tuple-element.65), calls=%async_computation.1 | async-start | bytes 1048576 | tf_op jit(solution)/shard_map/all_to_all | solution.py:482
  26.2 3.5 %pick.1 = (bf16[256,512]{1,0:T(8,128)(2,1)}, bf16[8,256,512]{2,1,0:T(8,128)(2,1)}) custom-call(bf16[2048,128]{1,0:T(8,128)(2,1)} %refs_0_, bf16[2048,128]{1,0:T(8,128)(2,1)} %refs_1_, bf16[2048,128]{1,0:T(8,128)(2,1)} %refs_2_, bf16[2048,128]{1,0:T(8,128)(2,1)} %refs_3_, bf16[2048,128]{1,0:T(8,128)(2,1)} %collective-permute-done.refs_4_, ...), custom_call_target="tpu_custom_call" | custom-call | flops 268435456 | bytes 6291456 | tf_op jit(solution)/shard_map/pick/pallas_call | solution.py:275
  33.7 2.9 %all-to-all-done.1.kv_ref = bf16[16,64,256]{2,1,0:T(8,128)(2,1)S(1)} async-done(((bf16[16,64,256]{2,1,0:T(8,128)(2,1)}), bf16[16,64,256]{2,1,0:T(8,128)(2,1)S(1)}, u32[]{:S(2)}, u32[]{:S(2)}) %all-to-all-start.1) | async-done | bytes 524320 | tf_op jit(solution)/shard_map/all_to_all | solution.py:482
  40.6 2.1 %collective-permute-start.4 = (bf16[1024,256]{1,0:T(8,128)(2,1)S(1)}, bf16[1024,256]{1,0:T(8,128)(2,1)S(1)}, u32[]{:S(2)}, u32[]{:S(2)}) collective-permute-start(bf16[1024,256]{1,0:T(8,128)(2,1)S(1)} %attend.1.mine_ref.d_ref), channel_id=1, source_target_pairs={{0,1},{1,0},{2,3},{3,2},{4,5},{5,4},{6,7},{7,6},{8,9},{9,8},{10,11... | collective-permute-start | bytes 1572872 | tf_op jit(solution)/shard_map/ppermute | solution.py:474
  42.8 1.5 %collective-permute-done.4.other_ref = bf16[1024,256]{1,0:T(8,128)(2,1)S(1)} collective-permute-done((bf16[1024,256]{1,0:T(8,128)(2,1)S(1)}, bf16[1024,256]{1,0:T(8,128)(2,1)S(1)}, u32[]{:S(2)}, u32[]{:S(2)}) %collective-permute-start.4) | collective-permute-done | bytes 524320 | tf_op jit(solution)/shard_map/ppermute | solution.py:474
  44.6 5.7 %collective-permute-start.5 = (bf16[512,256]{1,0:T(8,128)(2,1)S(1)}, bf16[512,256]{1,0:T(8,128)(2,1)S(1)}, u32[]{:S(2)}, u32[]{:S(2)}) collective-permute-start(bf16[512,256]{1,0:T(8,128)(2,1)S(1)} %far.1), channel_id=1, source_target_pairs={{0,2},{1,15},{2,4},{3,1},{4,6},{5,3},{6,8},{7,5},{8,10},{9,7},{10,... | collective-permute-start | bytes 786440 | tf_op jit(solution)/shard_map/ppermute | solution.py:474
  51.6 2.0 %collective-permute-done.5.came_ref = bf16[512,256]{1,0:T(8,128)(2,1)S(1)} collective-permute-done((bf16[512,256]{1,0:T(8,128)(2,1)S(1)}, bf16[512,256]{1,0:T(8,128)(2,1)S(1)}, u32[]{:S(2)}, u32[]{:S(2)}) %collective-permute-start.5) | collective-permute-done | bytes 262176 | tf_op jit(solution)/shard_map/ppermute | solution.py:474
  54.4 3.1 %collective-permute-start.10 = (bf16[512,256]{1,0:T(8,128)(2,1)}, bf16[512,256]{1,0:T(8,128)(2,1)S(1)}, u32[]{:S(2)}, u32[]{:S(2)}) collective-permute-start(bf16[512,256]{1,0:T(8,128)(2,1)} %shard_map.106), channel_id=1, source_target_pairs={{0,2},{1,15},{2,4},{3,1},{4,6},{5,3},{6,8},{7,5},{8,10},{9,7},{10,... | collective-permute-start | bytes 786440 | tf_op jit(solution)/shard_map/ppermute | solution.py:474
  58.8 3.7 %all-to-all-start.3 = ((bf16[16,128,128]{2,1,0:T(8,128)(2,1)}), bf16[16,128,128]{2,1,0:T(8,128)(2,1)S(1)}, u32[]{:S(2)}, u32[]{:S(2)}) async-start(bf16[16,128,128]{2,1,0:T(8,128)(2,1)} %weight_grad.1), calls=%async_computation.3 | async-start | bytes 1048576 | tf_op jit(solution)/shard_map/all_to_all | solution.py:493
  62.8 1.5 %collective-permute-start.11 = (bf16[512,256]{1,0:T(8,128)(2,1)S(1)}, bf16[512,256]{1,0:T(8,128)(2,1)S(1)}, u32[]{:S(2)}, u32[]{:S(2)}) collective-permute-start(bf16[512,256]{1,0:T(8,128)(2,1)S(1)} %shard_map.107), channel_id=1, source_target_pairs={{0,2},{1,15},{2,4},{3,1},{4,6},{5,3},{6,8},{7,5},{8,10},{9,7},{10,... | collective-permute-start | bytes 786440 | tf_op jit(solution)/shard_map/ppermute | solution.py:474
  64.3 3.9 %collective-permute-done.6.came_ref = bf16[512,256]{1,0:T(8,128)(2,1)S(1)} collective-permute-done((bf16[512,256]{1,0:T(8,128)(2,1)S(1)}, bf16[512,256]{1,0:T(8,128)(2,1)S(1)}, u32[]{:S(2)}, u32[]{:S(2)}) %collective-permute-start.6) | collective-permute-done | bytes 262176 | tf_op jit(solution)/shard_map/ppermute | solution.py:474
  69.6 1.4 %collective-permute-done.11.came_ref = bf16[512,256]{1,0:T(8,128)(2,1)S(1)} collective-permute-done((bf16[512,256]{1,0:T(8,128)(2,1)S(1)}, bf16[512,256]{1,0:T(8,128)(2,1)S(1)}, u32[]{:S(2)}, u32[]{:S(2)}) %collective-permute-start.11) | collective-permute-done | bytes 262176 | tf_op jit(solution)/shard_map/ppermute | solution.py:474
  71.1 1.5 %collective-permute-start.12 = (bf16[512,128]{1,0:T(8,128)(2,1)S(1)}, bf16[512,128]{1,0:T(8,128)(2,1)S(1)}, u32[]{:S(2)}, u32[]{:S(2)}) collective-permute-start(bf16[512,128]{1,0:T(8,128)(2,1)S(1)} %get-tuple-element.87), channel_id=1, source_target_pairs={{0,2},{1,15},{2,4},{3,1},{4,6},{5,3},{6,8},{7,5},{8,10},{9,7},{10,... | collective-permute-start | bytes 393224 | tf_op jit(solution)/shard_map/ppermute | solution.py:474
  72.6 2.3 %collective-permute-start.13 = (bf16[512,128]{1,0:T(8,128)(2,1)S(1)}, bf16[512,128]{1,0:T(8,128)(2,1)S(1)}, u32[]{:S(2)}, u32[]{:S(2)}) collective-permute-start(bf16[512,128]{1,0:T(8,128)(2,1)S(1)} %get-tuple-element.88), channel_id=1, source_target_pairs={{0,3},{1,14},{2,5},{3,0},{4,7},{5,2},{6,9},{7,4},{8,11},{9,6},{10,... | collective-permute-start | bytes 393224 | tf_op jit(solution)/shard_map/ppermute | solution.py:474
  75.5 3.4 %collective-permute-done.13.theirs_ref = bf16[512,128]{1,0:T(8,128)(2,1)S(1)} collective-permute-done((bf16[512,128]{1,0:T(8,128)(2,1)S(1)}, bf16[512,128]{1,0:T(8,128)(2,1)S(1)}, u32[]{:S(2)}, u32[]{:S(2)}) %collective-permute-start.13) | collective-permute-done | bytes 131104 | tf_op jit(solution)/shard_map/ppermute | solution.py:474
  80.3 6.9 %all-to-all-start.2 = ((bf16[16,64,128]{2,1,0:T(8,128)(2,1)}), bf16[16,64,128]{2,1,0:T(8,128)(2,1)S(1)}, u32[]{:S(2)}, u32[]{:S(2)}) async-start(bf16[16,64,128]{2,1,0:T(8,128)(2,1)} %finish_reads.1), calls=%async_computation.2 | async-start | bytes 524288 | tf_op jit(solution)/shard_map/all_to_all | solution.py:501
  88.1 1.6 %collective-permute-start.9 = (bf16[512,128]{1,0:T(8,128)(2,1)S(1)}, bf16[512,128]{1,0:T(8,128)(2,1)S(1)}, u32[]{:S(2)}, u32[]{:S(2)}) collective-permute-start(bf16[512,128]{1,0:T(8,128)(2,1)S(1)} %get-tuple-element.81), channel_id=1, source_target_pairs={{0,3},{1,14},{2,5},{3,0},{4,7},{5,2},{6,9},{7,4},{8,11},{9,6},{10,... | collective-permute-start | bytes 393224 | tf_op jit(solution)/shard_map/ppermute | solution.py:474
  91.4 2.6 %collective-permute-done.9.theirs_ref = bf16[512,128]{1,0:T(8,128)(2,1)S(1)} collective-permute-done((bf16[512,128]{1,0:T(8,128)(2,1)S(1)}, bf16[512,128]{1,0:T(8,128)(2,1)S(1)}, u32[]{:S(2)}, u32[]{:S(2)}) %collective-permute-start.9) | collective-permute-done | bytes 131104 | tf_op jit(solution)/shard_map/ppermute | solution.py:474
  94.8 1.6 %all-to-all-done.2.returned_ref = bf16[16,64,128]{2,1,0:T(8,128)(2,1)S(1)} async-done(((bf16[16,64,128]{2,1,0:T(8,128)(2,1)}), bf16[16,64,128]{2,1,0:T(8,128)(2,1)S(1)}, u32[]{:S(2)}, u32[]{:S(2)}) %all-to-all-start.2) | async-done | bytes 262176 | tf_op jit(solution)/shard_map/all_to_all | solution.py:501
  96.4 1.9 %collect.1 = f32[32,64,128]{2,1,0:T(8,128)} custom-call(s32[16]{0:T(128)S(1)} %copy-done.18, bf16[16,64,128]{2,1,0:T(8,128)(2,1)S(1)} %all-to-all-done.2.returned_ref), custom_call_target="tpu_custom_call" | custom-call | flops 1048576 | bytes 1048576 | tf_op jit(solution)/shard_map/collect/pallas_call | solution.py:433
  (73 shorter events, 21.8 us)
Async XLA Ops:
  0.6 16.7 %collective-permute-start = (bf16[2048,128]{1,0:T(8,128)(2,1)}, bf16[2048,128]{1,0:T(8,128)(2,1)}, u32[]{:S(2)}, u32[]{:S(2)}) collective-permute-start(bf16[2048,128]{1,0:T(8,128)(2,1)} %refs_0_), channel_id=1, source_target_pairs={{0,1},{1,0},{2,3},{3,2},{4,5},{5,4},{6,7},{7,6},{8,9},{9,8},{10,11... | collective-permute-start | bytes 1572872 | tf_op jit(solution)/shard_map/ppermute | solution.py:474
  3.9 13.4 %collective-permute-start.1 = (bf16[2048,128]{1,0:T(8,128)(2,1)}, bf16[2048,128]{1,0:T(8,128)(2,1)}, u32[]{:S(2)}, u32[]{:S(2)}) collective-permute-start(bf16[2048,128]{1,0:T(8,128)(2,1)} %refs_1_), channel_id=1, source_target_pairs={{0,1},{1,0},{2,3},{3,2},{4,5},{5,4},{6,7},{7,6},{8,9},{9,8},{10,11... | collective-permute-start | bytes 1572872 | tf_op jit(solution)/shard_map/ppermute | solution.py:474
  4.0 13.3 %collective-permute-start.2 = (bf16[2048,128]{1,0:T(8,128)(2,1)}, bf16[2048,128]{1,0:T(8,128)(2,1)}, u32[]{:S(2)}, u32[]{:S(2)}) collective-permute-start(bf16[2048,128]{1,0:T(8,128)(2,1)} %refs_2_), channel_id=1, source_target_pairs={{0,1},{1,0},{2,3},{3,2},{4,5},{5,4},{6,7},{7,6},{8,9},{9,8},{10,11... | collective-permute-start | bytes 1572872 | tf_op jit(solution)/shard_map/ppermute | solution.py:474
  4.4 12.9 %collective-permute-start.3 = (bf16[2048,128]{1,0:T(8,128)(2,1)}, bf16[2048,128]{1,0:T(8,128)(2,1)}, u32[]{:S(2)}, u32[]{:S(2)}) collective-permute-start(bf16[2048,128]{1,0:T(8,128)(2,1)} %refs_3_), channel_id=1, source_target_pairs={{0,1},{1,0},{2,3},{3,2},{4,5},{5,4},{6,7},{7,6},{8,9},{9,8},{10,11... | collective-permute-start | bytes 1572872 | tf_op jit(solution)/shard_map/ppermute | solution.py:474
  5.9 11.4 %all-to-all-start = ((s32[16,1,128]{2,1,0:T(1,128)}), s32[16,1,128]{2,1,0:T(1,128)S(1)}, u32[]{:S(2)}, u32[]{:S(2)}) async-start(s32[16,1,128]{2,1,0:T(1,128)} %get-tuple-element.47), calls=%async_computation | async-start | bytes 16384 | tf_op jit(solution)/shard_map/all_to_all | solution.py:467
  20.0 16.6 %all-to-all-start.1 = ((bf16[16,64,256]{2,1,0:T(8,128)(2,1)}), bf16[16,64,256]{2,1,0:T(8,128)(2,1)S(1)}, u32[]{:S(2)}, u32[]{:S(2)}) async-start(bf16[16,64,256]{2,1,0:T(8,128)(2,1)} %get-tuple-element.65), calls=%async_computation.1 | async-start | bytes 1048576 | tf_op jit(solution)/shard_map/all_to_all | solution.py:482
  30.7 13.5 %copy-start.7 = (bf16[256,512]{1,0:T(8,128)(2,1)S(1)}, bf16[256,512]{1,0:T(8,128)(2,1)}, u32[]{:S(2)}) copy-start(bf16[256,512]{1,0:T(8,128)(2,1)} %get-tuple-element.79.weight_ref) | copy-start | bytes 786436
  39.3 11.0 %copy-start.19 = (bf16[8,256,512]{2,1,0:T(8,128)(2,1)S(1)}, bf16[8,256,512]{2,1,0:T(8,128)(2,1)}, u32[]{:S(2)}) copy-start(bf16[8,256,512]{2,1,0:T(8,128)(2,1)} %get-tuple-element.74.held_ref) | copy-start | bytes 6291460
  40.6 3.7 %collective-permute-start.4 = (bf16[1024,256]{1,0:T(8,128)(2,1)S(1)}, bf16[1024,256]{1,0:T(8,128)(2,1)S(1)}, u32[]{:S(2)}, u32[]{:S(2)}) collective-permute-start(bf16[1024,256]{1,0:T(8,128)(2,1)S(1)} %attend.1.mine_ref.d_ref), channel_id=1, source_target_pairs={{0,1},{1,0},{2,3},{3,2},{4,5},{5,4},{6,7},{7,6},{8,9},{9,8},{10,11... | collective-permute-start | bytes 1572872 | tf_op jit(solution)/shard_map/ppermute | solution.py:474
  44.6 9.0 %collective-permute-start.5 = (bf16[512,256]{1,0:T(8,128)(2,1)S(1)}, bf16[512,256]{1,0:T(8,128)(2,1)S(1)}, u32[]{:S(2)}, u32[]{:S(2)}) collective-permute-start(bf16[512,256]{1,0:T(8,128)(2,1)S(1)} %far.1), channel_id=1, source_target_pairs={{0,2},{1,15},{2,4},{3,1},{4,6},{5,3},{6,8},{7,5},{8,10},{9,7},{10,... | collective-permute-start | bytes 786440 | tf_op jit(solution)/shard_map/ppermute | solution.py:474
  54.4 8.3 %collective-permute-start.10 = (bf16[512,256]{1,0:T(8,128)(2,1)}, bf16[512,256]{1,0:T(8,128)(2,1)S(1)}, u32[]{:S(2)}, u32[]{:S(2)}) collective-permute-start(bf16[512,256]{1,0:T(8,128)(2,1)} %shard_map.106), channel_id=1, source_target_pairs={{0,2},{1,15},{2,4},{3,1},{4,6},{5,3},{6,8},{7,5},{8,10},{9,7},{10,... | collective-permute-start | bytes 786440 | tf_op jit(solution)/shard_map/ppermute | solution.py:474
  58.8 12.2 %copy-start.6 = (bf16[512,256]{1,0:T(8,128)(2,1)S(1)}, bf16[512,256]{1,0:T(8,128)(2,1)}, u32[]{:S(2)}) copy-start(bf16[512,256]{1,0:T(8,128)(2,1)} %copy-done.5) | copy-start | bytes 786436
  58.8 20.1 %copy-start.10 = (bf16[512,128]{1,0:T(8,128)(2,1)S(1)}, bf16[512,128]{1,0:T(8,128)(2,1)}, u32[]{:S(2)}) copy-start(bf16[512,128]{1,0:T(8,128)(2,1)} %copy-done.9) | copy-start | bytes 393220
  58.8 21.4 %all-to-all-start.3 = ((bf16[16,128,128]{2,1,0:T(8,128)(2,1)}), bf16[16,128,128]{2,1,0:T(8,128)(2,1)S(1)}, u32[]{:S(2)}, u32[]{:S(2)}) async-start(bf16[16,128,128]{2,1,0:T(8,128)(2,1)} %weight_grad.1), calls=%async_computation.3 | async-start | bytes 1048576 | tf_op jit(solution)/shard_map/all_to_all | solution.py:493
  62.5 24.6 %copy-start.4 = (bf16[512,256]{1,0:T(8,128)(2,1)S(1)}, bf16[512,256]{1,0:T(8,128)(2,1)}, u32[]{:S(2)}) copy-start(bf16[512,256]{1,0:T(8,128)(2,1)} %copy-done.3) | copy-start | bytes 786436
  62.6 5.6 %collective-permute-start.6 = (bf16[512,256]{1,0:T(8,128)(2,1)S(1)}, bf16[512,256]{1,0:T(8,128)(2,1)S(1)}, u32[]{:S(2)}, u32[]{:S(2)}) collective-permute-start(bf16[512,256]{1,0:T(8,128)(2,1)S(1)} %shard_map.103), channel_id=1, source_target_pairs={{0,2},{1,15},{2,4},{3,1},{4,6},{5,3},{6,8},{7,5},{8,10},{9,7},{10,... | collective-permute-start | bytes 786440 | tf_op jit(solution)/shard_map/ppermute | solution.py:474
  62.8 8.2 %collective-permute-start.11 = (bf16[512,256]{1,0:T(8,128)(2,1)S(1)}, bf16[512,256]{1,0:T(8,128)(2,1)S(1)}, u32[]{:S(2)}, u32[]{:S(2)}) collective-permute-start(bf16[512,256]{1,0:T(8,128)(2,1)S(1)} %shard_map.107), channel_id=1, source_target_pairs={{0,2},{1,15},{2,4},{3,1},{4,6},{5,3},{6,8},{7,5},{8,10},{9,7},{10,... | collective-permute-start | bytes 786440 | tf_op jit(solution)/shard_map/ppermute | solution.py:474
  68.2 28.1 %copy-start.18 = (s32[16]{0:T(128)S(1)}, s32[16]{0:T(128)}, u32[]{:S(2)}) copy-start(s32[16]{0:T(128)} %get-tuple-element.82.wanted_ref) | copy-start | bytes 196
  68.3 18.8 %collective-permute-start.7 = (bf16[512,256]{1,0:T(8,128)(2,1)S(1)}, bf16[512,256]{1,0:T(8,128)(2,1)S(1)}, u32[]{:S(2)}, u32[]{:S(2)}) collective-permute-start(bf16[512,256]{1,0:T(8,128)(2,1)S(1)} %shard_map.104), channel_id=1, source_target_pairs={{0,2},{1,15},{2,4},{3,1},{4,6},{5,3},{6,8},{7,5},{8,10},{9,7},{10,... | collective-permute-start | bytes 786440 | tf_op jit(solution)/shard_map/ppermute | solution.py:474
  71.1 4.4 %collective-permute-start.12 = (bf16[512,128]{1,0:T(8,128)(2,1)S(1)}, bf16[512,128]{1,0:T(8,128)(2,1)S(1)}, u32[]{:S(2)}, u32[]{:S(2)}) collective-permute-start(bf16[512,128]{1,0:T(8,128)(2,1)S(1)} %get-tuple-element.87), channel_id=1, source_target_pairs={{0,2},{1,15},{2,4},{3,1},{4,6},{5,3},{6,8},{7,5},{8,10},{9,7},{10,... | collective-permute-start | bytes 393224 | tf_op jit(solution)/shard_map/ppermute | solution.py:474
  72.6 6.3 %collective-permute-start.13 = (bf16[512,128]{1,0:T(8,128)(2,1)S(1)}, bf16[512,128]{1,0:T(8,128)(2,1)S(1)}, u32[]{:S(2)}, u32[]{:S(2)}) collective-permute-start(bf16[512,128]{1,0:T(8,128)(2,1)S(1)} %get-tuple-element.88), channel_id=1, source_target_pairs={{0,3},{1,14},{2,5},{3,0},{4,7},{5,2},{6,9},{7,4},{8,11},{9,6},{10,... | collective-permute-start | bytes 393224 | tf_op jit(solution)/shard_map/ppermute | solution.py:474
  80.3 16.1 %all-to-all-start.2 = ((bf16[16,64,128]{2,1,0:T(8,128)(2,1)}), bf16[16,64,128]{2,1,0:T(8,128)(2,1)S(1)}, u32[]{:S(2)}, u32[]{:S(2)}) async-start(bf16[16,64,128]{2,1,0:T(8,128)(2,1)} %finish_reads.1), calls=%async_computation.2 | async-start | bytes 524288 | tf_op jit(solution)/shard_map/all_to_all | solution.py:501
  87.2 4.2 %collective-permute-start.8 = (bf16[512,128]{1,0:T(8,128)(2,1)S(1)}, bf16[512,128]{1,0:T(8,128)(2,1)S(1)}, u32[]{:S(2)}, u32[]{:S(2)}) collective-permute-start(bf16[512,128]{1,0:T(8,128)(2,1)S(1)} %get-tuple-element.80), channel_id=1, source_target_pairs={{0,2},{1,15},{2,4},{3,1},{4,6},{5,3},{6,8},{7,5},{8,10},{9,7},{10,... | collective-permute-start | bytes 393224 | tf_op jit(solution)/shard_map/ppermute | solution.py:474
  88.1 5.9 %collective-permute-start.9 = (bf16[512,128]{1,0:T(8,128)(2,1)S(1)}, bf16[512,128]{1,0:T(8,128)(2,1)S(1)}, u32[]{:S(2)}, u32[]{:S(2)}) collective-permute-start(bf16[512,128]{1,0:T(8,128)(2,1)S(1)} %get-tuple-element.81), channel_id=1, source_target_pairs={{0,3},{1,14},{2,5},{3,0},{4,7},{5,2},{6,9},{7,4},{8,11},{9,6},{10,... | collective-permute-start | bytes 393224 | tf_op jit(solution)/shard_map/ppermute | solution.py:474
  (15 other events, 34.3 us)

commit v3 on v2

--- a/solution.py
+++ b/solution.py
@@ -14,10 +14,13 @@
 BF16 = jnp.bfloat16
 F32 = jnp.float32
 NEAR = 40
+FAR = 16
 TOKENS = 40
 ATTEND = 8
 SERVE = 61
+PROJECT = 61
 GRAD = 40
+PICK = 61
 
 VMEM = pl.BlockSpec(memory_space=pltpu.VMEM)
 SMEM = pl.BlockSpec(memory_space=pltpu.SMEM)
@@ -87,6 +90,7 @@
         ],
         out_specs=pl.BlockSpec((tile, 2 * cols), lambda i: (i, 0)),
         out_shape=jax.ShapeDtypeStruct((rows, 2 * cols), BF16),
+        compiler_params=grant(PROJECT),
         cost_estimate=cost(4 * rows * width * cols, 2 * rows * width),
         name="project_store",
     )(store, w_key, w_value)
@@ -191,8 +195,7 @@
 
 
 def weight_grad_body(d_ref, x_ref, out_ref):
-    d_query = d_ref[: x_ref.shape[0], :DH]
-    flipped = d_query.astype(F32).T.astype(BF16)
+    flipped = d_ref[: x_ref.shape[0], :DH].astype(F32).T.astype(BF16)
     for j in range(out_ref.shape[0] // 2):
         both = nn(flipped, x_ref[:, 2 * j * DH : 2 * (j + 1) * DH]).astype(BF16)
         out_ref[2 * j] = both[:, :DH]
@@ -216,117 +219,91 @@
     return jnp.concatenate([mine_ref[side, :], other_ref[side, :]], axis=1)
 
 
-def place(chips):
+def first_row(chip, core, k, chips):
+    to = lax.rem(chip + k + core * (chips - 2 * k), chips)
+    return pl.multiple_of(to * 2 * DH, 2 * DH)
+
+
+FIRST = ((None, 4), (1, 3), (0, 3))
+REST = ((1, 2), (0, 2), (1, 1), (0, 1), (1, 0), (0, 0))
+
+
+def pick_body(chips, *refs):
+    weights, outs, sems = refs[:4], refs[4:8], refs[8:]
     at = lax.axis_index("tp")
-    core = lax.rem(at, 2)
+    here = lax.rem(at, 2)
     chip = lax.div(at, 2)
-
-    def first_row(k):
-        to = lax.rem(chip + k + core * (chips - 2 * k), chips)
-        return pl.multiple_of(to * 2 * DH, 2 * DH)
-
-    return core, chip, first_row
-
-
-JOBS = ((1, 3), (0, 3), (1, 2), (0, 2), (1, 1), (0, 1), (1, 0), (0, 0))
-
-
-def pick_body(chips, *refs):
-    weights, (far_ref, near_ref, far_sems, near_sems) = refs[:8], refs[8:]
-    core, chip, first_row = place(chips)
-
-    def source(half, piece):
-        return weights[(2 * half, 2 * half + 1, 4 + 2 * half, 5 + 2 * half)[piece]]
-
-    def far_copy(half, piece):
+    jobs = [(n, job) for n, table in enumerate((FIRST, REST)) for job in range(len(table))]
+
+    def copy(n, job, who, piece, half):
+        k = (FIRST, REST)[n][job][1]
+        core = here if who == 0 else 1 - here
+        home = pl.multiple_of((2 * chip + core) * DH, DH)
+        start, count = (first_row(chip, core, k, chips), 2 * DH) if k else (home, DH)
         return pltpu.make_async_copy(
-            source(half, piece).at[pl.ds(first_row(chips // 2), 2 * DH), :],
-            far_ref.at[:, pl.ds(piece * DH, DH)],
-            far_sems.at[piece],
+            weights[2 * half + piece].at[pl.ds(start, count), :],
+            outs[2 * n + who].at[job, pl.ds(0, count), pl.ds(piece * DH, DH)],
+            sems[n].at[who, piece, job],
         )
 
-    def near_copy(job, piece):
-        half, k = JOBS[job]
-        start = first_row(k) if k else pl.multiple_of((2 * chip + core) * DH, DH)
-        count = 2 * DH if k else DH
-        return pltpu.make_async_copy(
-            source(half, piece).at[pl.ds(start, count), :],
-            near_ref.at[job, pl.ds(0, count), pl.ds(piece * DH, DH)],
-            near_sems.at[job, piece],
-        )
-
-    for half in range(2):
-
-        @pl.when(core == half)
-        def _():
-            for piece in range(4):
-                far_copy(half, piece).start()
-
-    pairs = [(job, piece) for job in range(len(JOBS)) for piece in range(4)]
-    for job, piece in pairs:
-        near_copy(job, piece).start()
-    for piece in range(4):
-        far_copy(0, piece).wait()
-    for job, piece in pairs:
-        near_copy(job, piece).wait()
+    for n, job in jobs:
+        for who in range(2):
+            for piece in range(2):
+                half = (FIRST, REST)[n][job][0]
+                if half is not None:
+                    copy(n, job, who, piece, half).start()
+                    continue
+                for half in range(2):
+
+                    @pl.when(here == (half if who == 0 else 1 - half))
+                    def _():
+                        copy(n, job, who, piece, half).start()
+
+    for n, job in jobs:
+        for who in range(2):
+            for piece in range(2):
+                copy(n, job, who, piece, 0).wait()
 
 
 def pick(chips, weights):
+    shapes = [
+        jax.ShapeDtypeStruct((len(table), 2 * DH, 2 * DH), BF16) for table in (FIRST, REST)
+    ]
     return pl.pallas_call(
         functools.partial(pick_body, chips),
-        in_specs=[pl.BlockSpec(memory_space=pltpu.HBM)] * 8,
-        out_specs=[VMEM] * 2,
-        out_shape=[
-            jax.ShapeDtypeStruct((2 * DH, 4 * DH), BF16),
-            jax.ShapeDtypeStruct((len(JOBS), 2 * DH, 4 * DH), BF16),
-        ],
-        scratch_shapes=[pltpu.SemaphoreType.DMA((4,)), pltpu.SemaphoreType.DMA((len(JOBS), 4))],
+        in_specs=[pl.BlockSpec(memory_space=pltpu.HBM)] * 4,
+        out_specs=[VMEM] * 4,
+        out_shape=[shapes[0], shapes[0], shapes[1], shapes[1]],
+        scratch_shapes=[pltpu.SemaphoreType.DMA((2, 2, len(table))) for table in (FIRST, REST)],
+        compiler_params=grant(PICK),
         cost_estimate=cost(1 << 28, 6 << 20),
         name="pick",
     )(*weights)
 
 
-def far_body(mine_ref, other_ref, weight_ref, out_ref):
+def spread_body(table, mine_ref, other_ref, held_ref, lent_ref, *outs):
     core = lax.rem(lax.axis_index("tp"), 2)
-    tokens = out_ref.shape[0]
-    side = pl.ds(pl.multiple_of(core * tokens, tokens), tokens)
-    out_ref[...] = nt(both_heads(mine_ref, other_ref, side), weight_ref[...]).astype(BF16)
-
-
-def far(mine, other, weight):
+    tokens = mine_ref.shape[0] // 2
+    for job, (half, k) in enumerate(table):
+        start = core * tokens if half is None else half * tokens
+        side = pl.ds(pl.multiple_of(start, tokens), tokens)
+        count = 2 * DH if k else DH
+        right = jnp.concatenate([held_ref[job, :count, :], lent_ref[job, :count, :]], axis=1)
+        outs[job][...] = nt(both_heads(mine_ref, other_ref, side), right).astype(BF16)
+
+
+def spread(table, mine, other, held, lent, mib):
     tokens = mine.shape[0] // 2
     return pl.pallas_call(
-        far_body,
-        in_specs=[VMEM] * 3,
-        out_specs=VMEM,
-        out_shape=jax.ShapeDtypeStruct((tokens, 2 * DH), BF16),
-        compiler_params=grant(8),
-        cost_estimate=cost(16 * tokens * DH * DH, 1 << 20),
-        name="far",
-    )(mine, other, weight)
-
-
-def near_body(mine_ref, other_ref, held_ref, *outs):
-    tokens = mine_ref.shape[0] // 2
-    left = [both_heads(mine_ref, other_ref, slice(h * tokens, (h + 1) * tokens)) for h in range(2)]
-    for job, (half, k) in enumerate(JOBS):
-        right = held_ref[job, : 2 * DH if k else DH, :]
-        outs[job][...] = nt(left[half], right).astype(BF16)
-
-
-def near(mine, other, held):
-    tokens = mine.shape[0] // 2
-    return pl.pallas_call(
-        near_body,
-        in_specs=[VMEM] * 3,
-        out_specs=[VMEM] * len(JOBS),
+        functools.partial(spread_body, table),
+        in_specs=[VMEM] * 4,
+        out_specs=[VMEM] * len(table),
         out_shape=[
-            jax.ShapeDtypeStruct((tokens, 2 * DH if k else DH), BF16) for _, k in JOBS
+            jax.ShapeDtypeStruct((tokens, 2 * DH if k else DH), BF16) for _, k in table
         ],
-        compiler_params=grant(NEAR),
-        cost_estimate=cost(56 * 2 * tokens * DH * DH, 4 << 20),
-        name="near",
-    )(mine, other, held)
+        compiler_params=grant(mib),
+        cost_estimate=cost(16 * len(table) * tokens * DH * DH, 2 << 20),
+    )(mine, other, held, lent)
 
 
 def join_body(chosen, own_ref, came_ref, out_ref):
@@ -474,20 +451,23 @@
         return lax.ppermute(array, "tp", pairs)
 
     mine = (w_query, w_gate, w_key, w_value)
-    weights = mine + tuple(move(w, partner) for w in mine)
     projected = project_rows(store, w_key, w_value, 1024).reshape(pass_dev, PLEN, 2 * DH)
-    wanted, weights, projected = lax.optimization_barrier((wanted, weights, projected))
     served, wanted = serve(wanted, projected)
-    served, later, normed_later = lax.optimization_barrier((served, weights, normed))
+    served, mine, normed_later = lax.optimization_barrier((served, mine, normed))
     arrived = lax.all_to_all(served, "st", 0, 0, tiled=True)
-    queries, upstream, slope = project_tokens(normed_later, later[0], later[1], cotangent, 256)
-    weight4, held = pick(chips, later)
-    arrived, weight4 = lax.optimization_barrier((arrived, weight4))
+    held, gift, later_held, later_gift = pick(chips, mine)
+    lent = move(gift, partner)
+    later_lent = move(later_gift, partner)
+    queries, upstream, slope = project_tokens(normed_later, mine[0], mine[1], cotangent, 256)
+    arrived, held, later_held = lax.optimization_barrier((arrived, held, later_held))
     grads = attend(owners, queries, upstream, slope, arrived)
 
     other = move(grads, partner)
-    opposite = move(far(grads, other, weight4), along)
-    reads3, rows3, reads2, rows2, reads1, rows1, reads0, rows0 = near(grads, other, held)
+    opposite, reads3, rows3 = spread(FIRST, grads, other, held, lent, FAR)
+    opposite = move(opposite, along)
+    reads2, rows2, reads1, rows1, reads0, rows0 = spread(
+        REST, grads, other, later_held, later_lent, NEAR
+    )
     reads = move(join(reads3, opposite, 1), along)
     parts = weight_grad(grads, normed)
     parts = lax.all_to_all(parts, "st", 0, 0, tiled=True)

time: 99.1 us -> 100 us (level)
  Pallas kernels: 23.8 us -> 25.6 us
  starting transfers between devices: 45.7 us -> 44.2 us
    ppermute x14 -> x12, starting transfers between devices: 23.9 us -> 20 us  [move(): return lax.ppermute(array, 'tp', pairs)]
    all_to_all x1, starting transfers between devices: 5.06 us -> 7.58 us  [shards(): wanted = lax.all_to_all(table, 'st', 0, 0, tiled=True)]
    all_to_all x1, waiting for transfers between devices: 2.91 us -> 4.88 us  [shards(): arrived = lax.all_to_all(served, 'st', 0, 0, tiled=True)]
    all_to_all x1, waiting for transfers between devices: 1.55 us -> 0.03 us  [shards(): returned = lax.all_to_all(outgoing, 'st', 0, 0, tiled=True)]
    pallas_call x2, Pallas kernels: 1.61 us -> 2.75 us  [spread(): pl.pallas_call(functools.partial(spread_body, table), in_specs=[VMEM] * 4...]
    unnamed x42 -> x28, local copies, waits for them, and re-layouts: 6.33 us -> 6.58 us
    ppermute x14 -> x12, waiting for transfers between devices: 16.5 us -> 16.7 us  [move(): return lax.ppermute(array, 'tp', pairs)]
  transfers between devices with their start and end apart: 18 -> 16, of which waited for: 11 -> 8; matrix products, arithmetic and copies ran while one was open for 0% -> 0% of each run, Pallas kernels for 18% -> 18%
where the time goes in v3:
time: 100 us; the launch traced here: 99.5 us
  starting transfers between devices  44.2 us (44%)
  Pallas kernels  25.6 us (26%)
  waiting for transfers between devices  22.1 us (22%)
  local copies, waits for them, and re-layouts  6.58 us (7%)
  between operations  1.06 us (1%)
    ppermute x12, starting transfers between devices, move(): return lax.ppermute(array, 'tp', pairs)  20 us
    ppermute x12, waiting for transfers between devices, move(): return lax.ppermute(array, 'tp', pairs)  16.7 us
    all_to_all x1, starting transfers between devices, shards(): wanted = lax.all_to_all(table, 'st', 0, 0, tiled=True)  7.58 us
    all_to_all x1, starting transfers between devices, shards(): returned = lax.all_to_all(outgoing, 'st', 0, 0, tiled=True)  6.87 us
    unnamed x28, local copies, waits for them, and re-layouts  6.58 us
    all_to_all x1, starting transfers between devices, shards(): arrived = lax.all_to_all(served, 'st', 0, 0, tiled=True)  6.22 us
    pallas_call x1, Pallas kernels, project_rows(): pl.pallas_call(project_body, grid=(rows // tile,), in_specs=[pl.BlockSpec...  5.85 us
    all_to_all x1, waiting for transfers between devices, shards(): arrived = lax.all_to_all(served, 'st', 0, 0, tiled=True)  4.88 us
  transfers between devices with their start and end apart: 16, of which 8 were waited for; matrix products, arithmetic and copies ran while one was open for 0% of the time, Pallas kernels for 18%

profile of v3, /device:TPU:1, one launch (start us, length us, event | category | flops | bytes accessed | tf_op | source)
XLA Modules:
  0.0 99.5 jit_solution(11658050860273973786)
XLA Ops:
  0.7 1.4 %request.1 = (s32[16,1,128]{2,1,0:T(1,128)}, s32[8]{0:T(128)}) custom-call(s32[2,4]{1,0:T(2,128)} %bitcast.5), custom_call_target="tpu_custom_call" | custom-call | flops 65536 | bytes 65536 | tf_op jit(solution)/shard_map/request/pallas_call | solution.py:62
  2.1 7.6 %all-to-all-start = ((s32[16,1,128]{2,1,0:T(1,128)}), s32[16,1,128]{2,1,0:T(1,128)S(1)}, u32[]{:S(2)}, u32[]{:S(2)}) async-start(s32[16,1,128]{2,1,0:T(1,128)} %get-tuple-element.37), calls=%async_computation | async-start | bytes 16384 | tf_op jit(solution)/shard_map/all_to_all | solution.py:444
  9.7 5.8 %project_store.1 = bf16[2048,256]{1,0:T(8,128)(2,1)} custom-call(bf16[2048,2048]{1,0:T(8,128)(2,1)} %x_ref.2, bf16[2048,128]{1,0:T(8,128)(2,1)} %refs_2_, bf16[2048,128]{1,0:T(8,128)(2,1)} %refs_3_), custom_call_target="tpu_custom_call" | custom-call | flops 2147483648 | bytes 8388608 | tf_op jit(solution)/shard_map/project_store/pallas_call | solution.py:83
  16.7 2.1 %serve.1 = (bf16[16,64,256]{2,1,0:T(8,128)(2,1)}, s32[16]{0:T(128)}) custom-call(s32[16,1,128]{2,1,0:T(1,128)} %copy-done.13, bf16[32,64,256]{2,1,0:T(8,128)(2,1)} %bitcast.3), custom_call_target="tpu_custom_call" | custom-call | flops 1048576 | bytes 2097152 | tf_op jit(solution)/shard_map/serve/pallas_call | solution.py:108
  18.8 6.2 %all-to-all-start.1 = ((bf16[16,64,256]{2,1,0:T(8,128)(2,1)}), bf16[16,64,256]{2,1,0:T(8,128)(2,1)}, u32[]{:S(2)}, u32[]{:S(2)}) async-start(bf16[16,64,256]{2,1,0:T(8,128)(2,1)} %get-tuple-element.45), calls=%async_computation.1 | async-start | bytes 1048576 | tf_op jit(solution)/shard_map/all_to_all | solution.py:457
  25.0 3.3 %pick.1 = (bf16[3,256,256]{2,1,0:T(8,128)(2,1)}, bf16[3,256,256]{2,1,0:T(8,128)(2,1)}, bf16[6,256,256]{2,1,0:T(8,128)(2,1)}, bf16[6,256,256]{2,1,0:T(8,128)(2,1)}) custom-call(bf16[2048,128]{1,0:T(8,128)(2,1)} %refs_0_, bf16[2048,128]{1,0:T(8,128)(2,1)} %refs_1_, bf16[2048,128]{1,0:T(8,128)(2,1)} %refs_2_, bf16[2048,128]{1,0:T(8,128)(2,1)} %refs_3_), custom_call_target="tpu_custom_call" | custom-call | flops 268435456 | bytes 6291456 | tf_op jit(solution)/shard_map/pick/pallas_call | solution.py:272
  30.3 4.9 %all-to-all-done.1.kv_ref = bf16[16,64,256]{2,1,0:T(8,128)(2,1)} async-done(((bf16[16,64,256]{2,1,0:T(8,128)(2,1)}), bf16[16,64,256]{2,1,0:T(8,128)(2,1)}, u32[]{:S(2)}, u32[]{:S(2)}) %all-to-all-start.1) | async-done | bytes 524320 | tf_op jit(solution)/shard_map/all_to_all | solution.py:457
  35.2 1.8 %attend.1.mine_ref.d_ref = bf16[1024,256]{1,0:T(8,128)(2,1)S(1)} custom-call(s32[8]{0:T(128)S(1)} %copy-done.10, bf16[512,128]{1,0:T(8,128)(2,1)S(1)} %get-tuple-element.42.q_ref, bf16[512,128]{1,0:T(8,128)(2,1)S(1)} %get-tuple-element.43.up_ref, bf16[512,128]{1,0:T(8,128)(2,1)S(1)} %get-tuple-element.44.slope_ref, bf16[16,64,256]{2,1,0:T(8,128)(2,1)} %all-to-all-done.1.kv_ref), custom_call_target="tpu_custom_call" | custom-call | flops 117440512 | bytes 1048576 | tf_op jit(solution)/shard_map/attend/pallas_call | solution.py:186
  37.0 2.4 %collective-permute-start = (bf16[1024,256]{1,0:T(8,128)(2,1)S(1)}, bf16[1024,256]{1,0:T(8,128)(2,1)S(1)}, u32[]{:S(2)}, u32[]{:S(2)}) collective-permute-start(bf16[1024,256]{1,0:T(8,128)(2,1)S(1)} %attend.1.mine_ref.d_ref), channel_id=1, source_target_pairs={{0,1},{1,0},{2,3},{3,2},{4,5},{5,4},{6,7},{7,6},{8,9},{9,8},{10,11... | collective-permute-start | bytes 1572872 | tf_op jit(solution)/shard_map/ppermute | solution.py:451
  40.0 1.6 %collective-permute-done.2.lent_ref = bf16[3,256,256]{2,1,0:T(8,128)(2,1)S(1)} collective-permute-done((bf16[3,256,256]{2,1,0:T(8,128)(2,1)}, bf16[3,256,256]{2,1,0:T(8,128)(2,1)S(1)}, u32[]{:S(2)}, u32[]{:S(2)}) %collective-permute-start.2) | collective-permute-done | bytes 393248 | tf_op jit(solution)/shard_map/ppermute | solution.py:451
  43.2 5.7 %collective-permute-start.3 = (bf16[512,256]{1,0:T(8,128)(2,1)S(1)}, bf16[512,256]{1,0:T(8,128)(2,1)S(1)}, u32[]{:S(2)}, u32[]{:S(2)}) collective-permute-start(bf16[512,256]{1,0:T(8,128)(2,1)S(1)} %get-tuple-element.59), channel_id=1, source_target_pairs={{0,2},{1,15},{2,4},{3,1},{4,6},{5,3},{6,8},{7,5},{8,10},{9,7},{10,... | collective-permute-start | bytes 786440 | tf_op jit(solution)/shard_map/ppermute | solution.py:451
  48.8 3.3 %collective-permute-done.3.came_ref = bf16[512,256]{1,0:T(8,128)(2,1)S(1)} collective-permute-done((bf16[512,256]{1,0:T(8,128)(2,1)S(1)}, bf16[512,256]{1,0:T(8,128)(2,1)S(1)}, u32[]{:S(2)}, u32[]{:S(2)}) %collective-permute-start.3) | collective-permute-done | bytes 262176 | tf_op jit(solution)/shard_map/ppermute | solution.py:451
  53.0 3.1 %collective-permute-start.8 = (bf16[512,256]{1,0:T(8,128)(2,1)}, bf16[512,256]{1,0:T(8,128)(2,1)}, u32[]{:S(2)}, u32[]{:S(2)}) collective-permute-start(bf16[512,256]{1,0:T(8,128)(2,1)} %shard_map.108), channel_id=1, source_target_pairs={{0,2},{1,15},{2,4},{3,1},{4,6},{5,3},{6,8},{7,5},{8,10},{9,7},{10,... | collective-permute-start | bytes 786440 | tf_op jit(solution)/shard_map/ppermute | solution.py:451
  57.4 3.6 %all-to-all-start.3 = ((bf16[16,128,128]{2,1,0:T(8,128)(2,1)}), bf16[16,128,128]{2,1,0:T(8,128)(2,1)S(1)}, u32[]{:S(2)}, u32[]{:S(2)}) async-start(bf16[16,128,128]{2,1,0:T(8,128)(2,1)} %copy-done.3), calls=%async_computation.3 | async-start | bytes 1048576 | tf_op jit(solution)/shard_map/all_to_all | solution.py:473
  64.3 2.1 %shard_map.103 = (bf16[512,256]{1,0:T(8,128)(2,1)S(1)}, bf16[512,256]{1,0:T(8,128)(2,1)S(1)}, bf16[512,256]{1,0:T(8,128)(2,1)S(1)}, bf16[512,256]{1,0:T(8,128)(2...) custom-call(bf16[1024,256]{1,0:T(8,128)(2,1)S(1)} %attend.1.mine_ref.d_ref, ...), custom_call_target="tpu_custom_call" | custom-call | flops 805306368 | bytes 2097152 | tf_op jit(solution)/shard_map/pallas_call | solution.py:297
  69.0 4.1 %collective-permute-done.9.came_ref = bf16[512,256]{1,0:T(8,128)(2,1)S(1)} collective-permute-done((bf16[512,256]{1,0:T(8,128)(2,1)S(1)}, bf16[512,256]{1,0:T(8,128)(2,1)S(1)}, u32[]{:S(2)}, u32[]{:S(2)}) %collective-permute-start.9) | collective-permute-done | bytes 262176 | tf_op jit(solution)/shard_map/ppermute | solution.py:451
  73.2 1.5 %collective-permute-start.10 = (bf16[512,128]{1,0:T(8,128)(2,1)S(1)}, bf16[512,128]{1,0:T(8,128)(2,1)S(1)}, u32[]{:S(2)}, u32[]{:S(2)}) collective-permute-start(bf16[512,128]{1,0:T(8,128)(2,1)S(1)} %get-tuple-element.67), channel_id=1, source_target_pairs={{0,2},{1,15},{2,4},{3,1},{4,6},{5,3},{6,8},{7,5},{8,10},{9,7},{10,... | collective-permute-start | bytes 393224 | tf_op jit(solution)/shard_map/ppermute | solution.py:451
  74.7 2.1 %collective-permute-start.11 = (bf16[512,128]{1,0:T(8,128)(2,1)S(1)}, bf16[512,128]{1,0:T(8,128)(2,1)S(1)}, u32[]{:S(2)}, u32[]{:S(2)}) collective-permute-start(bf16[512,128]{1,0:T(8,128)(2,1)S(1)} %get-tuple-element.68), channel_id=1, source_target_pairs={{0,3},{1,14},{2,5},{3,0},{4,7},{5,2},{6,9},{7,4},{8,11},{9,6},{10,... | collective-permute-start | bytes 393224 | tf_op jit(solution)/shard_map/ppermute | solution.py:451
  77.1 3.7 %collective-permute-done.11.theirs_ref = bf16[512,128]{1,0:T(8,128)(2,1)S(1)} collective-permute-done((bf16[512,128]{1,0:T(8,128)(2,1)S(1)}, bf16[512,128]{1,0:T(8,128)(2,1)S(1)}, u32[]{:S(2)}, u32[]{:S(2)}) %collective-permute-start.11) | collective-permute-done | bytes 131104 | tf_op jit(solution)/shard_map/ppermute | solution.py:451
  80.8 1.3 %finish_reads.1 = bf16[16,64,128]{2,1,0:T(8,128)(2,1)} custom-call(s32[8]{0:T(128)S(1)} %copy-done.10, bf16[512,128]{1,0:T(8,128)(2,1)S(1)} %get-tuple-element.63.own_ref, bf16[512,128]{1,0:T(8,128)(2,1)S(1)} %collective-permute-done.10.ours_ref, bf16[512,128]{1,0:T(8,128)(2,1)S(1)} %collective-permute-done.11.theirs_ref), custom_call_target="tpu_custom_call" | custom-call | flops 1048576 | bytes 1048576 | tf_op jit(solution)/shard_map/finish_reads/pallas_call | solution.py:358
  82.1 6.9 %all-to-all-start.2 = ((bf16[16,64,128]{2,1,0:T(8,128)(2,1)}), bf16[16,64,128]{2,1,0:T(8,128)(2,1)S(1)}, u32[]{:S(2)}, u32[]{:S(2)}) async-start(bf16[16,64,128]{2,1,0:T(8,128)(2,1)} %finish_reads.1), calls=%async_computation.2 | async-start | bytes 524288 | tf_op jit(solution)/shard_map/all_to_all | solution.py:481
  90.0 2.3 %collective-permute-start.7 = (bf16[512,128]{1,0:T(8,128)(2,1)S(1)}, bf16[512,128]{1,0:T(8,128)(2,1)S(1)}, u32[]{:S(2)}, u32[]{:S(2)}) collective-permute-start(bf16[512,128]{1,0:T(8,128)(2,1)S(1)} %get-tuple-element.61), channel_id=1, source_target_pairs={{0,3},{1,14},{2,5},{3,0},{4,7},{5,2},{6,9},{7,4},{8,11},{9,6},{10,... | collective-permute-start | bytes 393224 | tf_op jit(solution)/shard_map/ppermute | solution.py:451
  93.1 3.6 %collective-permute-done.7.theirs_ref = bf16[512,128]{1,0:T(8,128)(2,1)S(1)} collective-permute-done((bf16[512,128]{1,0:T(8,128)(2,1)S(1)}, bf16[512,128]{1,0:T(8,128)(2,1)S(1)}, u32[]{:S(2)}, u32[]{:S(2)}) %collective-permute-start.7) | collective-permute-done | bytes 131104 | tf_op jit(solution)/shard_map/ppermute | solution.py:451
  97.4 1.9 %collect.1 = f32[32,64,128]{2,1,0:T(8,128)} custom-call(s32[16]{0:T(128)S(1)} %copy-done.11, bf16[16,64,128]{2,1,0:T(8,128)(2,1)S(1)} %all-to-all-done.2.returned_ref), custom_call_target="tpu_custom_call" | custom-call | flops 1048576 | bytes 1048576 | tf_op jit(solution)/shard_map/collect/pallas_call | solution.py:410
  (55 shorter events, 16.0 us)
Async XLA Ops:
  0.6 27.7 %copy-start = (bf16[512,2048]{1,0:T(8,128)(2,1)S(1)}, bf16[512,2048]{1,0:T(8,128)(2,1)}, u32[]{:S(2)}) copy-start(bf16[512,2048]{1,0:T(8,128)(2,1)} %x_ref.4) | copy-start | bytes 6291460
  0.6 27.7 %copy-start.1 = (bf16[2048,128]{1,0:T(8,128)(2,1)S(1)}, bf16[2048,128]{1,0:T(8,128)(2,1)}, u32[]{:S(2)}) copy-start(bf16[2048,128]{1,0:T(8,128)(2,1)} %refs_0_) | copy-start | bytes 1572868
  0.7 27.7 %copy-start.9 = (bf16[512,128]{1,0:T(8,128)(2,1)S(1)}, bf16[512,128]{1,0:T(8,128)(2,1)}, u32[]{:S(2)}) copy-start(bf16[512,128]{1,0:T(8,128)(2,1)} %cot_ref.1) | copy-start | bytes 393220
  2.1 14.0 %all-to-all-start = ((s32[16,1,128]{2,1,0:T(1,128)}), s32[16,1,128]{2,1,0:T(1,128)S(1)}, u32[]{:S(2)}, u32[]{:S(2)}) async-start(s32[16,1,128]{2,1,0:T(1,128)} %get-tuple-element.37), calls=%async_computation | async-start | bytes 16384 | tf_op jit(solution)/shard_map/all_to_all | solution.py:444
  9.7 25.5 %copy-start.10 = (s32[8]{0:T(128)S(1)}, s32[8]{0:T(128)}, u32[]{:S(2)}) copy-start(s32[8]{0:T(128)} %get-tuple-element.36.owner_ref) | copy-start | bytes 100
  18.8 16.4 %all-to-all-start.1 = ((bf16[16,64,256]{2,1,0:T(8,128)(2,1)}), bf16[16,64,256]{2,1,0:T(8,128)(2,1)}, u32[]{:S(2)}, u32[]{:S(2)}) async-start(bf16[16,64,256]{2,1,0:T(8,128)(2,1)} %get-tuple-element.45), calls=%async_computation.1 | async-start | bytes 1048576 | tf_op jit(solution)/shard_map/all_to_all | solution.py:457
  35.2 62.2 %copy-start.11 = (s32[16]{0:T(128)S(1)}, s32[16]{0:T(128)}, u32[]{:S(2)}) copy-start(s32[16]{0:T(128)} %get-tuple-element.62.wanted_ref) | copy-start | bytes 196
  37.0 4.5 %collective-permute-start = (bf16[1024,256]{1,0:T(8,128)(2,1)S(1)}, bf16[1024,256]{1,0:T(8,128)(2,1)S(1)}, u32[]{:S(2)}, u32[]{:S(2)}) collective-permute-start(bf16[1024,256]{1,0:T(8,128)(2,1)S(1)} %attend.1.mine_ref.d_ref), channel_id=1, source_target_pairs={{0,1},{1,0},{2,3},{3,2},{4,5},{5,4},{6,7},{7,6},{8,9},{9,8},{10,11... | collective-permute-start | bytes 1572872 | tf_op jit(solution)/shard_map/ppermute | solution.py:451
  39.5 2.1 %collective-permute-start.2 = (bf16[3,256,256]{2,1,0:T(8,128)(2,1)}, bf16[3,256,256]{2,1,0:T(8,128)(2,1)S(1)}, u32[]{:S(2)}, u32[]{:S(2)}) collective-permute-start(bf16[3,256,256]{2,1,0:T(8,128)(2,1)} %get-tuple-element.57), channel_id=1, source_target_pairs={{0,1},{1,0},{2,3},{3,2},{4,5},{5,4},{6,7},{7,6},{8,9},{9,8},{10,11... | collective-permute-start | bytes 1179656 | tf_op jit(solution)/shard_map/ppermute | solution.py:451
  39.6 22.5 %collective-permute-start.1 = (bf16[6,256,256]{2,1,0:T(8,128)(2,1)}, bf16[6,256,256]{2,1,0:T(8,128)(2,1)}, u32[]{:S(2)}, u32[]{:S(2)}) collective-permute-start(bf16[6,256,256]{2,1,0:T(8,128)(2,1)} %get-tuple-element.52), channel_id=1, source_target_pairs={{0,1},{1,0},{2,3},{3,2},{4,5},{5,4},{6,7},{7,6},{8,9},{9,8},{10,11... | collective-permute-start | bytes 2359304 | tf_op jit(solution)/shard_map/ppermute | solution.py:451
  42.6 10.4 %copy-start.4 = (bf16[1024,256]{1,0:T(8,128)(2,1)}, bf16[1024,256]{1,0:T(8,128)(2,1)S(1)}, u32[]{:S(2)}) copy-start(bf16[1024,256]{1,0:T(8,128)(2,1)S(1)} %collective-permute-done.other_ref) | copy-start | bytes 1572868
  43.2 9.8 %copy-start.7 = (bf16[512,256]{1,0:T(8,128)(2,1)}, bf16[512,256]{1,0:T(8,128)(2,1)S(1)}, u32[]{:S(2)}) copy-start(bf16[512,256]{1,0:T(8,128)(2,1)S(1)} %get-tuple-element.58.own_ref) | copy-start | bytes 786436
  43.2 9.0 %collective-permute-start.3 = (bf16[512,256]{1,0:T(8,128)(2,1)S(1)}, bf16[512,256]{1,0:T(8,128)(2,1)S(1)}, u32[]{:S(2)}, u32[]{:S(2)}) collective-permute-start(bf16[512,256]{1,0:T(8,128)(2,1)S(1)} %get-tuple-element.59), channel_id=1, source_target_pairs={{0,2},{1,15},{2,4},{3,1},{4,6},{5,3},{6,8},{7,5},{8,10},{9,7},{10,... | collective-permute-start | bytes 786440 | tf_op jit(solution)/shard_map/ppermute | solution.py:451
  53.0 13.5 %collective-permute-start.8 = (bf16[512,256]{1,0:T(8,128)(2,1)}, bf16[512,256]{1,0:T(8,128)(2,1)}, u32[]{:S(2)}, u32[]{:S(2)}) collective-permute-start(bf16[512,256]{1,0:T(8,128)(2,1)} %shard_map.108), channel_id=1, source_target_pairs={{0,2},{1,15},{2,4},{3,1},{4,6},{5,3},{6,8},{7,5},{8,10},{9,7},{10,... | collective-permute-start | bytes 786440 | tf_op jit(solution)/shard_map/ppermute | solution.py:451
  57.4 24.7 %all-to-all-start.3 = ((bf16[16,128,128]{2,1,0:T(8,128)(2,1)}), bf16[16,128,128]{2,1,0:T(8,128)(2,1)S(1)}, u32[]{:S(2)}, u32[]{:S(2)}) async-start(bf16[16,128,128]{2,1,0:T(8,128)(2,1)} %copy-done.3), calls=%async_computation.3 | async-start | bytes 1048576 | tf_op jit(solution)/shard_map/all_to_all | solution.py:473
  62.0 6.1 %collective-permute-start.4 = (bf16[512,256]{1,0:T(8,128)(2,1)S(1)}, bf16[512,256]{1,0:T(8,128)(2,1)S(1)}, u32[]{:S(2)}, u32[]{:S(2)}) collective-permute-start(bf16[512,256]{1,0:T(8,128)(2,1)S(1)} %shard_map.105), channel_id=1, source_target_pairs={{0,2},{1,15},{2,4},{3,1},{4,6},{5,3},{6,8},{7,5},{8,10},{9,7},{10,... | collective-permute-start | bytes 786440 | tf_op jit(solution)/shard_map/ppermute | solution.py:451
  63.1 1.1 %copy-start.12 = (bf16[6,256,256]{2,1,0:T(8,128)(2,1)S(1)}, bf16[6,256,256]{2,1,0:T(8,128)(2,1)}, u32[]{:S(2)}) copy-start(bf16[6,256,256]{2,1,0:T(8,128)(2,1)} %get-tuple-element.51.held_ref) | copy-start | bytes 2359300
  67.5 5.6 %collective-permute-start.9 = (bf16[512,256]{1,0:T(8,128)(2,1)S(1)}, bf16[512,256]{1,0:T(8,128)(2,1)S(1)}, u32[]{:S(2)}, u32[]{:S(2)}) collective-permute-start(bf16[512,256]{1,0:T(8,128)(2,1)S(1)} %shard_map.109), channel_id=1, source_target_pairs={{0,2},{1,15},{2,4},{3,1},{4,6},{5,3},{6,8},{7,5},{8,10},{9,7},{10,... | collective-permute-start | bytes 786440 | tf_op jit(solution)/shard_map/ppermute | solution.py:451
  68.1 20.8 %collective-permute-start.5 = (bf16[512,256]{1,0:T(8,128)(2,1)S(1)}, bf16[512,256]{1,0:T(8,128)(2,1)S(1)}, u32[]{:S(2)}, u32[]{:S(2)}) collective-permute-start(bf16[512,256]{1,0:T(8,128)(2,1)S(1)} %shard_map.106), channel_id=1, source_target_pairs={{0,2},{1,15},{2,4},{3,1},{4,6},{5,3},{6,8},{7,5},{8,10},{9,7},{10,... | collective-permute-start | bytes 786440 | tf_op jit(solution)/shard_map/ppermute | solution.py:451
  73.2 3.9 %collective-permute-start.10 = (bf16[512,128]{1,0:T(8,128)(2,1)S(1)}, bf16[512,128]{1,0:T(8,128)(2,1)S(1)}, u32[]{:S(2)}, u32[]{:S(2)}) collective-permute-start(bf16[512,128]{1,0:T(8,128)(2,1)S(1)} %get-tuple-element.67), channel_id=1, source_target_pairs={{0,2},{1,15},{2,4},{3,1},{4,6},{5,3},{6,8},{7,5},{8,10},{9,7},{10,... | collective-permute-start | bytes 393224 | tf_op jit(solution)/shard_map/ppermute | solution.py:451
  74.7 6.1 %collective-permute-start.11 = (bf16[512,128]{1,0:T(8,128)(2,1)S(1)}, bf16[512,128]{1,0:T(8,128)(2,1)S(1)}, u32[]{:S(2)}, u32[]{:S(2)}) collective-permute-start(bf16[512,128]{1,0:T(8,128)(2,1)S(1)} %get-tuple-element.68), channel_id=1, source_target_pairs={{0,3},{1,14},{2,5},{3,0},{4,7},{5,2},{6,9},{7,4},{8,11},{9,6},{10,... | collective-permute-start | bytes 393224 | tf_op jit(solution)/shard_map/ppermute | solution.py:451
  82.1 15.3 %all-to-all-start.2 = ((bf16[16,64,128]{2,1,0:T(8,128)(2,1)}), bf16[16,64,128]{2,1,0:T(8,128)(2,1)S(1)}, u32[]{:S(2)}, u32[]{:S(2)}) async-start(bf16[16,64,128]{2,1,0:T(8,128)(2,1)} %finish_reads.1), calls=%async_computation.2 | async-start | bytes 524288 | tf_op jit(solution)/shard_map/all_to_all | solution.py:481
  89.1 4.0 %collective-permute-start.6 = (bf16[512,128]{1,0:T(8,128)(2,1)S(1)}, bf16[512,128]{1,0:T(8,128)(2,1)S(1)}, u32[]{:S(2)}, u32[]{:S(2)}) collective-permute-start(bf16[512,128]{1,0:T(8,128)(2,1)S(1)} %get-tuple-element.60), channel_id=1, source_target_pairs={{0,2},{1,15},{2,4},{3,1},{4,6},{5,3},{6,8},{7,5},{8,10},{9,7},{10,... | collective-permute-start | bytes 393224 | tf_op jit(solution)/shard_map/ppermute | solution.py:451
  90.0 6.7 %collective-permute-start.7 = (bf16[512,128]{1,0:T(8,128)(2,1)S(1)}, bf16[512,128]{1,0:T(8,128)(2,1)S(1)}, u32[]{:S(2)}, u32[]{:S(2)}) collective-permute-start(bf16[512,128]{1,0:T(8,128)(2,1)S(1)} %get-tuple-element.61), channel_id=1, source_target_pairs={{0,3},{1,14},{2,5},{3,0},{4,7},{5,2},{6,9},{7,4},{8,11},{9,6},{10,... | collective-permute-start | bytes 393224 | tf_op jit(solution)/shard_map/ppermute | solution.py:451
  (6 other events, 5.4 us)

commit v4 on v3

--- a/solution.py
+++ b/solution.py
@@ -382,37 +382,22 @@
     )(own, ours, theirs)
 
 
-def collect_body(wanted_ref, returned_ref, out_ref, sum_ref, sems):
-    pieces = sems.shape[0]
-    count = out_ref.shape[0] // pieces
-
-    def leave(i):
-        at = pl.ds(i * count, count)
-        return pltpu.make_async_copy(sum_ref.at[at], out_ref.at[at], sems.at[i])
-
-    for i in range(pieces):
-        sum_ref[i * count : (i + 1) * count] = jnp.zeros((count,) + sum_ref.shape[1:], F32)
-        for s in range(returned_ref.shape[0]):
-            passage = wanted_ref[s]
-
-            @pl.when((passage >= i * count) & (passage < (i + 1) * count))
-            def _():
-                at = jnp.clip(passage, i * count, (i + 1) * count - 1)
-                sum_ref[at] = sum_ref[at] + returned_ref[s].astype(F32)
-
-        leave(i).start()
-    for i in range(pieces):
-        leave(i).wait()
+def collect_body(wanted_ref, returned_ref, out_ref):
+    out_ref[...] = jnp.zeros_like(out_ref)
+    for s in range(returned_ref.shape[0]):
+
+        @pl.when(wanted_ref[s] >= 0)
+        def _():
+            at = jnp.clip(wanted_ref[s], 0, out_ref.shape[0] - 1)
+            out_ref[at] = out_ref[at] + returned_ref[s].astype(F32)
 
 
 def collect(wanted, returned, passages):
-    pieces = 4
     return pl.pallas_call(
         collect_body,
         in_specs=[SMEM, VMEM],
-        out_specs=pl.BlockSpec(memory_space=pltpu.HBM),
+        out_specs=VMEM,
         out_shape=jax.ShapeDtypeStruct((passages, PLEN, DH), F32),
-        scratch_shapes=[pltpu.VMEM((passages, PLEN, DH), F32), pltpu.SemaphoreType.DMA((pieces,))],
         compiler_params=grant(8),
         cost_estimate=cost(1 << 20, 1 << 20),
         name="collect",

time: 100 us -> 100 us (level)
  no operation moved by 1% of the time
where the time goes in v4:
time: 100 us; the launch traced here: 99.2 us
  starting transfers between devices  44.2 us (44%)
  Pallas kernels  25.4 us (25%)
  waiting for transfers between devices  22.1 us (22%)
  local copies, waits for them, and re-layouts  6.58 us (7%)
    ppermute x12, starting transfers between devices, move(): return lax.ppermute(array, 'tp', pairs)  20 us
    ppermute x12, waiting for transfers between devices, move(): return lax.ppermute(array, 'tp', pairs)  16.7 us
    all_to_all x1, starting transfers between devices, shards(): wanted = lax.all_to_all(table, 'st', 0, 0, tiled=True)  7.58 us
    all_to_all x1, starting transfers between devices, shards(): returned = lax.all_to_all(outgoing, 'st', 0, 0, tiled=True)  6.88 us
    unnamed x28, local copies, waits for them, and re-layouts  6.58 us
    all_to_all x1, starting transfers between devices, shards(): arrived = lax.all_to_all(served, 'st', 0, 0, tiled=True)  6.22 us
    pallas_call x1, Pallas kernels, project_rows(): pl.pallas_call(project_body, grid=(rows // tile,), in_specs=[pl.BlockSpec...  5.85 us
    all_to_all x1, waiting for transfers between devices, shards(): arrived = lax.all_to_all(served, 'st', 0, 0, tiled=True)  4.88 us
  transfers between devices with their start and end apart: 16, of which 8 were waited for; matrix products, arithmetic and copies ran while one was open for 0% of the time, Pallas kernels for 18%

profile of v4, /device:TPU:1, one launch (start us, length us, event | category | flops | bytes accessed | tf_op | source)
XLA Modules:
  0.0 99.2 jit_solution(951395274679136614)
XLA Ops:
  0.7 1.4 %request.1 = (s32[16,1,128]{2,1,0:T(1,128)}, s32[8]{0:T(128)}) custom-call(s32[2,4]{1,0:T(2,128)} %bitcast.5), custom_call_target="tpu_custom_call" | custom-call | flops 65536 | bytes 65536 | tf_op jit(solution)/shard_map/request/pallas_call | solution.py:62
  2.1 7.6 %all-to-all-start = ((s32[16,1,128]{2,1,0:T(1,128)}), s32[16,1,128]{2,1,0:T(1,128)S(1)}, u32[]{:S(2)}, u32[]{:S(2)}) async-start(s32[16,1,128]{2,1,0:T(1,128)} %get-tuple-element.37), calls=%async_computation | async-start | bytes 16384 | tf_op jit(solution)/shard_map/all_to_all | solution.py:429
  9.7 5.8 %project_store.1 = bf16[2048,256]{1,0:T(8,128)(2,1)} custom-call(bf16[2048,2048]{1,0:T(8,128)(2,1)} %x_ref.2, bf16[2048,128]{1,0:T(8,128)(2,1)} %refs_2_, bf16[2048,128]{1,0:T(8,128)(2,1)} %refs_3_), custom_call_target="tpu_custom_call" | custom-call | flops 2147483648 | bytes 8388608 | tf_op jit(solution)/shard_map/project_store/pallas_call | solution.py:83
  16.7 2.1 %serve.1 = (bf16[16,64,256]{2,1,0:T(8,128)(2,1)}, s32[16]{0:T(128)}) custom-call(s32[16,1,128]{2,1,0:T(1,128)} %copy-done.13, bf16[32,64,256]{2,1,0:T(8,128)(2,1)} %bitcast.3), custom_call_target="tpu_custom_call" | custom-call | flops 1048576 | bytes 2097152 | tf_op jit(solution)/shard_map/serve/pallas_call | solution.py:108
  18.8 6.2 %all-to-all-start.1 = ((bf16[16,64,256]{2,1,0:T(8,128)(2,1)}), bf16[16,64,256]{2,1,0:T(8,128)(2,1)}, u32[]{:S(2)}, u32[]{:S(2)}) async-start(bf16[16,64,256]{2,1,0:T(8,128)(2,1)} %get-tuple-element.45), calls=%async_computation.1 | async-start | bytes 1048576 | tf_op jit(solution)/shard_map/all_to_all | solution.py:442
  25.0 3.3 %pick.1 = (bf16[3,256,256]{2,1,0:T(8,128)(2,1)}, bf16[3,256,256]{2,1,0:T(8,128)(2,1)}, bf16[6,256,256]{2,1,0:T(8,128)(2,1)}, bf16[6,256,256]{2,1,0:T(8,128)(2,1)}) custom-call(bf16[2048,128]{1,0:T(8,128)(2,1)} %refs_0_, bf16[2048,128]{1,0:T(8,128)(2,1)} %refs_1_, bf16[2048,128]{1,0:T(8,128)(2,1)} %refs_2_, bf16[2048,128]{1,0:T(8,128)(2,1)} %refs_3_), custom_call_target="tpu_custom_call" | custom-call | flops 268435456 | bytes 6291456 | tf_op jit(solution)/shard_map/pick/pallas_call | solution.py:272
  30.3 4.9 %all-to-all-done.1.kv_ref = bf16[16,64,256]{2,1,0:T(8,128)(2,1)} async-done(((bf16[16,64,256]{2,1,0:T(8,128)(2,1)}), bf16[16,64,256]{2,1,0:T(8,128)(2,1)}, u32[]{:S(2)}, u32[]{:S(2)}) %all-to-all-start.1) | async-done | bytes 524320 | tf_op jit(solution)/shard_map/all_to_all | solution.py:442
  35.2 1.8 %attend.1.mine_ref.d_ref = bf16[1024,256]{1,0:T(8,128)(2,1)S(1)} custom-call(s32[8]{0:T(128)S(1)} %copy-done.10, bf16[512,128]{1,0:T(8,128)(2,1)S(1)} %get-tuple-element.42.q_ref, bf16[512,128]{1,0:T(8,128)(2,1)S(1)} %get-tuple-element.43.up_ref, bf16[512,128]{1,0:T(8,128)(2,1)S(1)} %get-tuple-element.44.slope_ref, bf16[16,64,256]{2,1,0:T(8,128)(2,1)} %all-to-all-done.1.kv_ref), custom_call_target="tpu_custom_call" | custom-call | flops 117440512 | bytes 1048576 | tf_op jit(solution)/shard_map/attend/pallas_call | solution.py:186
  37.0 2.4 %collective-permute-start = (bf16[1024,256]{1,0:T(8,128)(2,1)S(1)}, bf16[1024,256]{1,0:T(8,128)(2,1)S(1)}, u32[]{:S(2)}, u32[]{:S(2)}) collective-permute-start(bf16[1024,256]{1,0:T(8,128)(2,1)S(1)} %attend.1.mine_ref.d_ref), channel_id=1, source_target_pairs={{0,1},{1,0},{2,3},{3,2},{4,5},{5,4},{6,7},{7,6},{8,9},{9,8},{10,11... | collective-permute-start | bytes 1572872 | tf_op jit(solution)/shard_map/ppermute | solution.py:436
  40.0 1.6 %collective-permute-done.2.lent_ref = bf16[3,256,256]{2,1,0:T(8,128)(2,1)S(1)} collective-permute-done((bf16[3,256,256]{2,1,0:T(8,128)(2,1)}, bf16[3,256,256]{2,1,0:T(8,128)(2,1)S(1)}, u32[]{:S(2)}, u32[]{:S(2)}) %collective-permute-start.2) | collective-permute-done | bytes 393248 | tf_op jit(solution)/shard_map/ppermute | solution.py:436
  43.2 5.7 %collective-permute-start.3 = (bf16[512,256]{1,0:T(8,128)(2,1)S(1)}, bf16[512,256]{1,0:T(8,128)(2,1)S(1)}, u32[]{:S(2)}, u32[]{:S(2)}) collective-permute-start(bf16[512,256]{1,0:T(8,128)(2,1)S(1)} %get-tuple-element.59), channel_id=1, source_target_pairs={{0,2},{1,15},{2,4},{3,1},{4,6},{5,3},{6,8},{7,5},{8,10},{9,7},{10,... | collective-permute-start | bytes 786440 | tf_op jit(solution)/shard_map/ppermute | solution.py:436
  48.8 3.3 %collective-permute-done.3.came_ref = bf16[512,256]{1,0:T(8,128)(2,1)S(1)} collective-permute-done((bf16[512,256]{1,0:T(8,128)(2,1)S(1)}, bf16[512,256]{1,0:T(8,128)(2,1)S(1)}, u32[]{:S(2)}, u32[]{:S(2)}) %collective-permute-start.3) | collective-permute-done | bytes 262176 | tf_op jit(solution)/shard_map/ppermute | solution.py:436
  53.0 3.1 %collective-permute-start.8 = (bf16[512,256]{1,0:T(8,128)(2,1)}, bf16[512,256]{1,0:T(8,128)(2,1)}, u32[]{:S(2)}, u32[]{:S(2)}) collective-permute-start(bf16[512,256]{1,0:T(8,128)(2,1)} %shard_map.108), channel_id=1, source_target_pairs={{0,2},{1,15},{2,4},{3,1},{4,6},{5,3},{6,8},{7,5},{8,10},{9,7},{10,... | collective-permute-start | bytes 786440 | tf_op jit(solution)/shard_map/ppermute | solution.py:436
  57.4 3.6 %all-to-all-start.3 = ((bf16[16,128,128]{2,1,0:T(8,128)(2,1)}), bf16[16,128,128]{2,1,0:T(8,128)(2,1)S(1)}, u32[]{:S(2)}, u32[]{:S(2)}) async-start(bf16[16,128,128]{2,1,0:T(8,128)(2,1)} %copy-done.3), calls=%async_computation.3 | async-start | bytes 1048576 | tf_op jit(solution)/shard_map/all_to_all | solution.py:458
  64.3 2.1 %shard_map.103 = (bf16[512,256]{1,0:T(8,128)(2,1)S(1)}, bf16[512,256]{1,0:T(8,128)(2,1)S(1)}, bf16[512,256]{1,0:T(8,128)(2,1)S(1)}, bf16[512,256]{1,0:T(8,128)(2...) custom-call(bf16[1024,256]{1,0:T(8,128)(2,1)S(1)} %attend.1.mine_ref.d_ref, ...), custom_call_target="tpu_custom_call" | custom-call | flops 805306368 | bytes 2097152 | tf_op jit(solution)/shard_map/pallas_call | solution.py:297
  69.0 4.1 %collective-permute-done.9.came_ref = bf16[512,256]{1,0:T(8,128)(2,1)S(1)} collective-permute-done((bf16[512,256]{1,0:T(8,128)(2,1)S(1)}, bf16[512,256]{1,0:T(8,128)(2,1)S(1)}, u32[]{:S(2)}, u32[]{:S(2)}) %collective-permute-start.9) | collective-permute-done | bytes 262176 | tf_op jit(solution)/shard_map/ppermute | solution.py:436
  73.2 1.5 %collective-permute-start.10 = (bf16[512,128]{1,0:T(8,128)(2,1)S(1)}, bf16[512,128]{1,0:T(8,128)(2,1)S(1)}, u32[]{:S(2)}, u32[]{:S(2)}) collective-permute-start(bf16[512,128]{1,0:T(8,128)(2,1)S(1)} %get-tuple-element.67), channel_id=1, source_target_pairs={{0,2},{1,15},{2,4},{3,1},{4,6},{5,3},{6,8},{7,5},{8,10},{9,7},{10,... | collective-permute-start | bytes 393224 | tf_op jit(solution)/shard_map/ppermute | solution.py:436
  74.7 2.1 %collective-permute-start.11 = (bf16[512,128]{1,0:T(8,128)(2,1)S(1)}, bf16[512,128]{1,0:T(8,128)(2,1)S(1)}, u32[]{:S(2)}, u32[]{:S(2)}) collective-permute-start(bf16[512,128]{1,0:T(8,128)(2,1)S(1)} %get-tuple-element.68), channel_id=1, source_target_pairs={{0,3},{1,14},{2,5},{3,0},{4,7},{5,2},{6,9},{7,4},{8,11},{9,6},{10,... | collective-permute-start | bytes 393224 | tf_op jit(solution)/shard_map/ppermute | solution.py:436
  77.1 3.7 %collective-permute-done.11.theirs_ref = bf16[512,128]{1,0:T(8,128)(2,1)S(1)} collective-permute-done((bf16[512,128]{1,0:T(8,128)(2,1)S(1)}, bf16[512,128]{1,0:T(8,128)(2,1)S(1)}, u32[]{:S(2)}, u32[]{:S(2)}) %collective-permute-start.11) | collective-permute-done | bytes 131104 | tf_op jit(solution)/shard_map/ppermute | solution.py:436
  80.8 1.3 %finish_reads.1 = bf16[16,64,128]{2,1,0:T(8,128)(2,1)} custom-call(s32[8]{0:T(128)S(1)} %copy-done.10, bf16[512,128]{1,0:T(8,128)(2,1)S(1)} %get-tuple-element.63.own_ref, bf16[512,128]{1,0:T(8,128)(2,1)S(1)} %collective-permute-done.10.ours_ref, bf16[512,128]{1,0:T(8,128)(2,1)S(1)} %collective-permute-done.11.theirs_ref), custom_call_target="tpu_custom_call" | custom-call | flops 1048576 | bytes 1048576 | tf_op jit(solution)/shard_map/finish_reads/pallas_call | solution.py:358
  82.1 6.9 %all-to-all-start.2 = ((bf16[16,64,128]{2,1,0:T(8,128)(2,1)}), bf16[16,64,128]{2,1,0:T(8,128)(2,1)S(1)}, u32[]{:S(2)}, u32[]{:S(2)}) async-start(bf16[16,64,128]{2,1,0:T(8,128)(2,1)} %finish_reads.1), calls=%async_computation.2 | async-start | bytes 524288 | tf_op jit(solution)/shard_map/all_to_all | solution.py:466
  90.0 2.3 %collective-permute-start.7 = (bf16[512,128]{1,0:T(8,128)(2,1)S(1)}, bf16[512,128]{1,0:T(8,128)(2,1)S(1)}, u32[]{:S(2)}, u32[]{:S(2)}) collective-permute-start(bf16[512,128]{1,0:T(8,128)(2,1)S(1)} %get-tuple-element.61), channel_id=1, source_target_pairs={{0,3},{1,14},{2,5},{3,0},{4,7},{5,2},{6,9},{7,4},{8,11},{9,6},{10,... | collective-permute-start | bytes 393224 | tf_op jit(solution)/shard_map/ppermute | solution.py:436
  93.1 3.6 %collective-permute-done.7.theirs_ref = bf16[512,128]{1,0:T(8,128)(2,1)S(1)} collective-permute-done((bf16[512,128]{1,0:T(8,128)(2,1)S(1)}, bf16[512,128]{1,0:T(8,128)(2,1)S(1)}, u32[]{:S(2)}, u32[]{:S(2)}) %collective-permute-start.7) | collective-permute-done | bytes 131104 | tf_op jit(solution)/shard_map/ppermute | solution.py:436
  97.4 1.8 %collect.1 = f32[32,64,128]{2,1,0:T(8,128)} custom-call(s32[16]{0:T(128)S(1)} %copy-done.11, bf16[16,64,128]{2,1,0:T(8,128)(2,1)S(1)} %all-to-all-done.2.returned_ref), custom_call_target="tpu_custom_call" | custom-call | flops 1048576 | bytes 1048576 | tf_op jit(solution)/shard_map/collect/pallas_call | solution.py:396
  (55 shorter events, 16.0 us)
Async XLA Ops:
  0.6 27.7 %copy-start = (bf16[512,2048]{1,0:T(8,128)(2,1)S(1)}, bf16[512,2048]{1,0:T(8,128)(2,1)}, u32[]{:S(2)}) copy-start(bf16[512,2048]{1,0:T(8,128)(2,1)} %x_ref.4) | copy-start | bytes 6291460
  0.6 27.7 %copy-start.1 = (bf16[2048,128]{1,0:T(8,128)(2,1)S(1)}, bf16[2048,128]{1,0:T(8,128)(2,1)}, u32[]{:S(2)}) copy-start(bf16[2048,128]{1,0:T(8,128)(2,1)} %refs_0_) | copy-start | bytes 1572868
  0.7 27.7 %copy-start.9 = (bf16[512,128]{1,0:T(8,128)(2,1)S(1)}, bf16[512,128]{1,0:T(8,128)(2,1)}, u32[]{:S(2)}) copy-start(bf16[512,128]{1,0:T(8,128)(2,1)} %cot_ref.1) | copy-start | bytes 393220
  2.1 14.0 %all-to-all-start = ((s32[16,1,128]{2,1,0:T(1,128)}), s32[16,1,128]{2,1,0:T(1,128)S(1)}, u32[]{:S(2)}, u32[]{:S(2)}) async-start(s32[16,1,128]{2,1,0:T(1,128)} %get-tuple-element.37), calls=%async_computation | async-start | bytes 16384 | tf_op jit(solution)/shard_map/all_to_all | solution.py:429
  9.7 25.5 %copy-start.10 = (s32[8]{0:T(128)S(1)}, s32[8]{0:T(128)}, u32[]{:S(2)}) copy-start(s32[8]{0:T(128)} %get-tuple-element.36.owner_ref) | copy-start | bytes 100
  18.8 16.4 %all-to-all-start.1 = ((bf16[16,64,256]{2,1,0:T(8,128)(2,1)}), bf16[16,64,256]{2,1,0:T(8,128)(2,1)}, u32[]{:S(2)}, u32[]{:S(2)}) async-start(bf16[16,64,256]{2,1,0:T(8,128)(2,1)} %get-tuple-element.45), calls=%async_computation.1 | async-start | bytes 1048576 | tf_op jit(solution)/shard_map/all_to_all | solution.py:442
  35.2 62.2 %copy-start.11 = (s32[16]{0:T(128)S(1)}, s32[16]{0:T(128)}, u32[]{:S(2)}) copy-start(s32[16]{0:T(128)} %get-tuple-element.62.wanted_ref) | copy-start | bytes 196
  37.0 4.5 %collective-permute-start = (bf16[1024,256]{1,0:T(8,128)(2,1)S(1)}, bf16[1024,256]{1,0:T(8,128)(2,1)S(1)}, u32[]{:S(2)}, u32[]{:S(2)}) collective-permute-start(bf16[1024,256]{1,0:T(8,128)(2,1)S(1)} %attend.1.mine_ref.d_ref), channel_id=1, source_target_pairs={{0,1},{1,0},{2,3},{3,2},{4,5},{5,4},{6,7},{7,6},{8,9},{9,8},{10,11... | collective-permute-start | bytes 1572872 | tf_op jit(solution)/shard_map/ppermute | solution.py:436
  39.5 2.1 %collective-permute-start.2 = (bf16[3,256,256]{2,1,0:T(8,128)(2,1)}, bf16[3,256,256]{2,1,0:T(8,128)(2,1)S(1)}, u32[]{:S(2)}, u32[]{:S(2)}) collective-permute-start(bf16[3,256,256]{2,1,0:T(8,128)(2,1)} %get-tuple-element.57), channel_id=1, source_target_pairs={{0,1},{1,0},{2,3},{3,2},{4,5},{5,4},{6,7},{7,6},{8,9},{9,8},{10,11... | collective-permute-start | bytes 1179656 | tf_op jit(solution)/shard_map/ppermute | solution.py:436
  39.6 22.5 %collective-permute-start.1 = (bf16[6,256,256]{2,1,0:T(8,128)(2,1)}, bf16[6,256,256]{2,1,0:T(8,128)(2,1)}, u32[]{:S(2)}, u32[]{:S(2)}) collective-permute-start(bf16[6,256,256]{2,1,0:T(8,128)(2,1)} %get-tuple-element.52), channel_id=1, source_target_pairs={{0,1},{1,0},{2,3},{3,2},{4,5},{5,4},{6,7},{7,6},{8,9},{9,8},{10,11... | collective-permute-start | bytes 2359304 | tf_op jit(solution)/shard_map/ppermute | solution.py:436
  42.6 10.4 %copy-start.4 = (bf16[1024,256]{1,0:T(8,128)(2,1)}, bf16[1024,256]{1,0:T(8,128)(2,1)S(1)}, u32[]{:S(2)}) copy-start(bf16[1024,256]{1,0:T(8,128)(2,1)S(1)} %collective-permute-done.other_ref) | copy-start | bytes 1572868
  43.2 9.8 %copy-start.7 = (bf16[512,256]{1,0:T(8,128)(2,1)}, bf16[512,256]{1,0:T(8,128)(2,1)S(1)}, u32[]{:S(2)}) copy-start(bf16[512,256]{1,0:T(8,128)(2,1)S(1)} %get-tuple-element.58.own_ref) | copy-start | bytes 786436
  43.2 9.0 %collective-permute-start.3 = (bf16[512,256]{1,0:T(8,128)(2,1)S(1)}, bf16[512,256]{1,0:T(8,128)(2,1)S(1)}, u32[]{:S(2)}, u32[]{:S(2)}) collective-permute-start(bf16[512,256]{1,0:T(8,128)(2,1)S(1)} %get-tuple-element.59), channel_id=1, source_target_pairs={{0,2},{1,15},{2,4},{3,1},{4,6},{5,3},{6,8},{7,5},{8,10},{9,7},{10,... | collective-permute-start | bytes 786440 | tf_op jit(solution)/shard_map/ppermute | solution.py:436
  53.0 13.5 %collective-permute-start.8 = (bf16[512,256]{1,0:T(8,128)(2,1)}, bf16[512,256]{1,0:T(8,128)(2,1)}, u32[]{:S(2)}, u32[]{:S(2)}) collective-permute-start(bf16[512,256]{1,0:T(8,128)(2,1)} %shard_map.108), channel_id=1, source_target_pairs={{0,2},{1,15},{2,4},{3,1},{4,6},{5,3},{6,8},{7,5},{8,10},{9,7},{10,... | collective-permute-start | bytes 786440 | tf_op jit(solution)/shard_map/ppermute | solution.py:436
  57.4 24.7 %all-to-all-start.3 = ((bf16[16,128,128]{2,1,0:T(8,128)(2,1)}), bf16[16,128,128]{2,1,0:T(8,128)(2,1)S(1)}, u32[]{:S(2)}, u32[]{:S(2)}) async-start(bf16[16,128,128]{2,1,0:T(8,128)(2,1)} %copy-done.3), calls=%async_computation.3 | async-start | bytes 1048576 | tf_op jit(solution)/shard_map/all_to_all | solution.py:458
  62.0 6.1 %collective-permute-start.4 = (bf16[512,256]{1,0:T(8,128)(2,1)S(1)}, bf16[512,256]{1,0:T(8,128)(2,1)S(1)}, u32[]{:S(2)}, u32[]{:S(2)}) collective-permute-start(bf16[512,256]{1,0:T(8,128)(2,1)S(1)} %shard_map.105), channel_id=1, source_target_pairs={{0,2},{1,15},{2,4},{3,1},{4,6},{5,3},{6,8},{7,5},{8,10},{9,7},{10,... | collective-permute-start | bytes 786440 | tf_op jit(solution)/shard_map/ppermute | solution.py:436
  63.1 1.1 %copy-start.12 = (bf16[6,256,256]{2,1,0:T(8,128)(2,1)S(1)}, bf16[6,256,256]{2,1,0:T(8,128)(2,1)}, u32[]{:S(2)}) copy-start(bf16[6,256,256]{2,1,0:T(8,128)(2,1)} %get-tuple-element.51.held_ref) | copy-start | bytes 2359300
  67.5 5.6 %collective-permute-start.9 = (bf16[512,256]{1,0:T(8,128)(2,1)S(1)}, bf16[512,256]{1,0:T(8,128)(2,1)S(1)}, u32[]{:S(2)}, u32[]{:S(2)}) collective-permute-start(bf16[512,256]{1,0:T(8,128)(2,1)S(1)} %shard_map.109), channel_id=1, source_target_pairs={{0,2},{1,15},{2,4},{3,1},{4,6},{5,3},{6,8},{7,5},{8,10},{9,7},{10,... | collective-permute-start | bytes 786440 | tf_op jit(solution)/shard_map/ppermute | solution.py:436
  68.1 20.8 %collective-permute-start.5 = (bf16[512,256]{1,0:T(8,128)(2,1)S(1)}, bf16[512,256]{1,0:T(8,128)(2,1)S(1)}, u32[]{:S(2)}, u32[]{:S(2)}) collective-permute-start(bf16[512,256]{1,0:T(8,128)(2,1)S(1)} %shard_map.106), channel_id=1, source_target_pairs={{0,2},{1,15},{2,4},{3,1},{4,6},{5,3},{6,8},{7,5},{8,10},{9,7},{10,... | collective-permute-start | bytes 786440 | tf_op jit(solution)/shard_map/ppermute | solution.py:436
  73.2 3.9 %collective-permute-start.10 = (bf16[512,128]{1,0:T(8,128)(2,1)S(1)}, bf16[512,128]{1,0:T(8,128)(2,1)S(1)}, u32[]{:S(2)}, u32[]{:S(2)}) collective-permute-start(bf16[512,128]{1,0:T(8,128)(2,1)S(1)} %get-tuple-element.67), channel_id=1, source_target_pairs={{0,2},{1,15},{2,4},{3,1},{4,6},{5,3},{6,8},{7,5},{8,10},{9,7},{10,... | collective-permute-start | bytes 393224 | tf_op jit(solution)/shard_map/ppermute | solution.py:436
  74.7 6.1 %collective-permute-start.11 = (bf16[512,128]{1,0:T(8,128)(2,1)S(1)}, bf16[512,128]{1,0:T(8,128)(2,1)S(1)}, u32[]{:S(2)}, u32[]{:S(2)}) collective-permute-start(bf16[512,128]{1,0:T(8,128)(2,1)S(1)} %get-tuple-element.68), channel_id=1, source_target_pairs={{0,3},{1,14},{2,5},{3,0},{4,7},{5,2},{6,9},{7,4},{8,11},{9,6},{10,... | collective-permute-start | bytes 393224 | tf_op jit(solution)/shard_map/ppermute | solution.py:436
  82.1 15.3 %all-to-all-start.2 = ((bf16[16,64,128]{2,1,0:T(8,128)(2,1)}), bf16[16,64,128]{2,1,0:T(8,128)(2,1)S(1)}, u32[]{:S(2)}, u32[]{:S(2)}) async-start(bf16[16,64,128]{2,1,0:T(8,128)(2,1)} %finish_reads.1), calls=%async_computation.2 | async-start | bytes 524288 | tf_op jit(solution)/shard_map/all_to_all | solution.py:466
  89.1 4.0 %collective-permute-start.6 = (bf16[512,128]{1,0:T(8,128)(2,1)S(1)}, bf16[512,128]{1,0:T(8,128)(2,1)S(1)}, u32[]{:S(2)}, u32[]{:S(2)}) collective-permute-start(bf16[512,128]{1,0:T(8,128)(2,1)S(1)} %get-tuple-element.60), channel_id=1, source_target_pairs={{0,2},{1,15},{2,4},{3,1},{4,6},{5,3},{6,8},{7,5},{8,10},{9,7},{10,... | collective-permute-start | bytes 393224 | tf_op jit(solution)/shard_map/ppermute | solution.py:436
  90.0 6.7 %collective-permute-start.7 = (bf16[512,128]{1,0:T(8,128)(2,1)S(1)}, bf16[512,128]{1,0:T(8,128)(2,1)S(1)}, u32[]{:S(2)}, u32[]{:S(2)}) collective-permute-start(bf16[512,128]{1,0:T(8,128)(2,1)S(1)} %get-tuple-element.61), channel_id=1, source_target_pairs={{0,3},{1,14},{2,5},{3,0},{4,7},{5,2},{6,9},{7,4},{8,11},{9,6},{10,... | collective-permute-start | bytes 393224 | tf_op jit(solution)/shard_map/ppermute | solution.py:436
  (6 other events, 5.4 us)
